TPU v7x, 32 devices: a whole 2x2x4 slice. The times are simulated.
32 devices in a mesh: sp: 16 (over z, y, x), tp: 2 (over core).
Axes of the slice: x: 2, y: 2, z: 4, core: 2. Of those that a mesh axis runs over, the one named last changes fastest.
Arguments:
- resid: bfloat16 [3072, 2048], P('sp'), may hold values from -6 to 6
- queries: bfloat16 [3072, 1024], P('sp', 'tp'), may hold values from -6.5 to 6.5
- keys: bfloat16 [3072, 1024], P('sp', 'tp'), may hold values from -6.5 to 6.5
- values: bfloat16 [3072, 1024], P('sp', 'tp'), may hold values from -6 to 6
- lambdas: float32 [8], P('tp'), may hold values from 0.3 to 0.8
- head_gain: float32 [128], replicated, may hold values from 0.1 to 1.9
- out_weight: bfloat16 [1024, 2048], P('tp'), may hold values from -0.1875 to 0.1875
- norm_gain: float32 [2048], replicated, may hold values from 0.1 to 1.9
- gate_weight: bfloat16 [2048, 5632], P('sp', 'tp'), may hold values from -0.125 to 0.125
- up_weight: bfloat16 [2048, 5632], P('sp', 'tp'), may hold values from -0.125 to 0.125
- down_weight: bfloat16 [5632, 2048], P('tp', 'sp'), may hold values from -0.078125 to 0.078125
Outputs:
- result: bfloat16 [3072, 2048], P('sp')
All inputs are finite; a program needn't handle non-finite values.
Results may differ from a plain program's by a relative error of at most 0.014.
Values may be sent and summed in bfloat16 or wider, within the bound.
No kernel may reach another device: no remote copies, remote signals or barrier semaphores. Data moves between devices by JAX's collectives and lax.ppermute only.
A program may use at most 128 MiB of HBM per device.

v0:
```python
import jax
import jax.numpy as jnp
from jax import lax
from jax.sharding import PartitionSpec as P

QK = 64
VD = 128


def rms_rows(first, norm_gain):
    return (
        first * lax.rsqrt(jnp.mean(first * first, axis=-1, keepdims=True) + 1e-06) * norm_gain
    ).astype(jnp.bfloat16)


def local(
    resid,
    queries,
    keys,
    values,
    lambdas,
    head_gain,
    out_weight,
    norm_gain,
    gate_weight,
    up_weight,
    down_weight,
):
    tok_rows = queries.shape[0]
    local_heads = lambdas.shape[0]
    model_width = resid.shape[1]
    offset = lax.axis_index("sp") * tok_rows
    query_four = queries.reshape(tok_rows, local_heads, 2, QK)
    score_scale = QK ** (-0.5)
    query_pos = offset + lax.iota(jnp.int32, tok_rows)
    last_query = offset + tok_rows - 1

    def update(fold_state, key_part, value_part, key_pos):
        run_max, run_sum, run_acc = fold_state
        scores = (
            jnp.einsum("qhcd,khcd->chqk", query_four, key_part, preferred_element_type=jnp.float32)
            * score_scale
        )
        causal_mask = key_pos[None, :] <= query_pos[:, None]
        scores = jnp.where(causal_mask, scores, -1e30)
        new_max = jnp.maximum(run_max, jnp.max(scores, axis=-1))
        expo = jnp.where(causal_mask, jnp.exp(scores - new_max[..., None]), 0.0)
        factor = jnp.exp(run_max - new_max)
        new_sum = run_sum * factor + jnp.sum(expo, axis=-1)
        new_acc = run_acc * factor[..., None] + jnp.einsum(
            "chqk,khd->chqd",
            expo.astype(jnp.bfloat16),
            value_part,
            preferred_element_type=jnp.float32,
        )
        return (new_max, new_sum, new_acc)

    initial = (
        jnp.full((2, local_heads, tok_rows), -1e30, jnp.float32),
        jnp.zeros((2, local_heads, tok_rows), jnp.float32),
        jnp.zeros((2, local_heads, tok_rows, VD), jnp.float32),
    )
    key_rows = lax.all_gather(keys, "sp", axis=0, tiled=True)
    value_rows = lax.all_gather(values, "sp", axis=0, tiled=True)
    key_count = key_rows.shape[0]
    key_span = key_count
    while key_span > 1024 and key_span % 2 == 0:
        key_span = key_span // 2

    def one_span(span_index, inner_state):
        span_start = span_index * key_span
        key_part = lax.dynamic_slice_in_dim(key_rows, span_start, key_span, 0).reshape(
            key_span, local_heads, 2, QK
        )
        value_part = lax.dynamic_slice_in_dim(value_rows, span_start, key_span, 0).reshape(
            key_span, local_heads, VD
        )
        key_pos = span_start + lax.iota(jnp.int32, key_span)
        return update(inner_state, key_part, value_part, key_pos)

    def run_spans(inner_state):
        return lax.fori_loop(0, key_count // key_span, one_span, inner_state)

    def keep_state(inner_state):
        return inner_state

    final_max, final_sum, final_acc = lax.cond(
        jnp.int32(0) <= last_query, run_spans, keep_state, initial
    )
    ratio = final_acc / final_sum[..., None]
    mixed_heads = ratio[0] - lambdas[:, None, None] * ratio[1]
    head_out = (
        mixed_heads
        * lax.rsqrt(jnp.mean(mixed_heads * mixed_heads, axis=-1, keepdims=True) + 1e-05)
        * head_gain
    ).astype(jnp.bfloat16)
    out_three = out_weight.reshape(local_heads, VD, model_width)
    own_count = tok_rows // lax.axis_size("tp")
    branch = lax.psum_scatter(
        jnp.einsum("hqd,hde->qe", head_out, out_three, preferred_element_type=jnp.float32).astype(
            jnp.bfloat16
        ),
        "tp",
        scatter_dimension=0,
        tiled=True,
    ).astype(jnp.float32)
    resid_own = lax.dynamic_slice_in_dim(resid, lax.axis_index("tp") * own_count, own_count, 0)
    first = resid_own.astype(jnp.float32) + branch
    normed_all = lax.all_gather(rms_rows(first, norm_gain), "tp", axis=0, tiled=True)
    gate_act = jnp.dot(
        normed_all,
        lax.all_gather(gate_weight, "sp", axis=0, tiled=True),
        preferred_element_type=jnp.float32,
    )
    up_act = jnp.dot(
        normed_all,
        lax.all_gather(up_weight, "sp", axis=0, tiled=True),
        preferred_element_type=jnp.float32,
    )
    hidden = (jax.nn.silu(gate_act) * up_act).astype(jnp.bfloat16)
    terms = jnp.dot(
        hidden,
        lax.all_gather(down_weight, "sp", axis=1, tiled=True),
        preferred_element_type=jnp.float32,
    )
    mixer = lax.psum_scatter(
        terms.astype(jnp.bfloat16), "tp", scatter_dimension=0, tiled=True
    ).astype(jnp.float32)
    finished = (first + 0.5 * mixer).astype(jnp.bfloat16)
    return lax.all_gather(finished, "tp", axis=0, tiled=True)


def solution(mesh):
    return jax.shard_map(
        local,
        mesh=mesh,
        in_specs=(
            P("sp", None),
            P("sp", "tp"),
            P("sp", "tp"),
            P("sp", "tp"),
            P("tp"),
            P(),
            P("tp", None),
            P(),
            P("sp", "tp"),
            P("sp", "tp"),
            P("tp", "sp"),
        ),
        out_specs=P("sp", None),
        check_vma=False,
    )
```

profile of v0, /device:TPU:0, one launch (start us, length us, event | category | flops | bytes accessed | tf_op | source)
XLA Modules:
  0.0 741.6 jit_solution(319168003058939454)
XLA Ops:
  8.1 72.7 %all-gather.6.cloned.1.call-done = bf16[3072,512]{1,0:T(8,128)(2,1)} async-done(((bf16[192,512]{1,0:T(8,128)(2,1)}), bf16[3072,512]{1,0:T(8,128)(2,1)}) %all-gather.6.cloned.1.call-update) | async-done | bytes 3145744 | tf_op jit(solution)/shard_map/all_gather | solution.py:63
  80.7 69.2 %all-gather.8.cloned.1.call-done = bf16[3072,512]{1,0:T(8,128)(2,1)} async-done(((bf16[192,512]{1,0:T(8,128)(2,1)}), bf16[3072,512]{1,0:T(8,128)(2,1)}) %all-gather.8.cloned.1.call-update) | async-done | bytes 3145744 | tf_op jit(solution)/shard_map/all_gather | solution.py:64
  150.0 78.7 %conditional.1 = (f32[2,4,192]{2,1,0:T(4,128)}, f32[2,4,192,128]{3,2,0,1:T(8,128)}) conditional(s32[]{:T(128)} %convert_element_type.38, () %tuple.27, (bf16[192,512]{1,0:T(8,128)(2,1)}, s32[]{:T(128)}, s32[192]{0:T(256)S(1)}, bf16[3072,512]{1,0:T(8,128)(2,1)}, bf16[3072,512]{1,0:T(8,128)(2,1)}) %tuple.28), branch_computations={%region_0.0_spmd, %region_1.6_spmd} | conditional | flops 464347584 | bytes 25131568 | solution.py:87
  151.1 77.6 %while.17 = (s32[]{:T(128)}, f32[2,4,192]{2,1,0:T(4,128)S(1)}, f32[2,4,192]{2,1,0:T(4,128)}, f32[2,4,192,128]{3,2,0,1:T(8,128)}, s32[192]{0:T(256)S(1)}, /*index...) while((s32[]{:T(128)}, f32[2,4,192]{2,1,0:T(4,128)S(1)}, ...), condition=%wide.region_5.5_spmd.clone, body=%wide.region_2.4_spmd.clone.sunk | while | flops 464347392 | bytes 24343476 | solution.py:82
  155.9 4.2 fusion.41
  160.2 4.3 fusion.42
  166.3 3.6 fusion.44
  174.7 4.2 fusion.41
  178.9 4.3 fusion.42
  185.7 3.7 fusion.44
  194.3 4.2 fusion.41
  198.5 4.3 fusion.42
  205.3 3.7 fusion.44
  213.9 4.2 fusion.41
  218.1 4.3 fusion.42
  224.9 3.7 fusion.44
  234.5 5.1 reduce-scatter.3.cloned.1.call-done
  242.0 2.5 all_gather.23
  244.5 140.3 %all-gather.10.cloned.1.call-done = bf16[2048,2816]{1,0:T(8,128)(2,1)} async-done(((bf16[128,2816]{1,0:T(8,128)(2,1)}), bf16[2048,2816]{1,0:T(8,128)(2,1)}) %all-gather.10.cloned.1.call-update) | async-done | bytes 11534352 | tf_op jit(solution)/shard_map/all_gather | solution.py:112
  384.7 8.3 %fusion.22 = f32[192,2816]{1,0:T(8,128)} fusion(bf16[192,2048]{1,0:T(8,128)(2,1)} %all_gather.23, bf16[2048,2816]{1,0:T(8,128)(2,1)} %all-gather.10.cloned.1.call-done), kind=kOutput, calls=%fused_computation.42 | convolution fusion | flops 2214592512 | bytes 14483456 | tf_op jit(solution)/shard_map/dot_general | solution.py:110
  393.1 133.9 %all-gather.12.cloned.1.call-done = bf16[2048,2816]{1,0:T(8,128)(2,1)} async-done(((bf16[128,2816]{1,0:T(8,128)(2,1)}), bf16[2048,2816]{1,0:T(8,128)(2,1)}) %all-gather.12.cloned.1.call-update) | async-done | bytes 11534352 | tf_op jit(solution)/shard_map/all_gather | solution.py:117
  527.0 182.8 %all-gather.14.cloned.1.call-done = bf16[2816,2048]{1,0:T(8,128)(2,1)} async-done(((bf16[2816,128]{1,0:T(8,128)(2,1)}), bf16[2816,2048]{1,0:T(8,128)(2,1)}) %all-gather.14.cloned.1.call-update) | async-done | bytes 11534352 | tf_op jit(solution)/shard_map/all_gather | solution.py:123
  709.8 14.0 %convolution_convert_fusion = bf16[192,2048]{1,0:T(8,128)(2,1)} fusion(bf16[2816,2048]{1,0:T(8,128)(2,1)} %all-gather.14.cloned.1.call-done, bf16[192,2048]{1,0:T(8,128)(2,1)} %all_gather.23, bf16[2048,2816]{1,0:T(8,128)(2,1)} %all-gather.12.cloned.1.call-done, f32[192,2816]{1,0:T(8,128)} %fusion.22), kind=kOutput, calls=%fused_computation.25 | convolution fusion | flops 4432822272 | bytes 26804224 | tf_op jit(solution)/shard_map/dot_general | solution.py:121
  723.8 6.5 reduce-scatter.5.cloned.1.call-done
  (80 shorter events, 43.6 us)
Async XLA Ops:
  6.5 224.6 %copy-start = (bf16[512,2048]{1,0:T(8,128)(2,1)S(1)}, bf16[512,2048]{1,0:T(8,128)(2,1)}, u32[]{:S(2)}) copy-start(bf16[512,2048]{1,0:T(8,128)(2,1)} %param.21) | copy-start | bytes 6291460
  6.5 74.2 %all-gather.6.cloned.1.call-start = ((), (), s32[]{:S(2)}) async-start(), calls=%async_computation.2 | async-start | bytes 3342336 | tf_op jit(solution)/shard_map/all_gather | solution.py:63
  7.3 142.7 %all-gather.8.cloned.1.call-start = ((), (), s32[]{:S(2)}) async-start(), calls=%async_computation.3 | async-start | bytes 3342336 | tf_op jit(solution)/shard_map/all_gather | solution.py:64
  8.0 231.6 %reduce-scatter.3.cloned.1.call-start = ((), (), s32[]{:S(2)}) async-start(), calls=%async_computation.4 | async-start | bytes 1179648 | tf_op jit(solution)/shard_map/reduce_scatter | solution.py:99
  149.9 80.8 %copy-start.4 = (f32[4]{0:T(128)S(1)}, f32[4]{0:T(128)}, u32[]{:S(2)}) copy-start(f32[4]{0:T(128)} %param.19) | copy-start | bytes 52
  149.9 81.2 %copy-start.5 = (f32[128]{0:T(128)S(1)}, f32[128]{0:T(128)}, u32[]{:S(2)}) copy-start(f32[128]{0:T(128)} %param.20) | copy-start | bytes 1540
  231.1 8.5 %copy-start.2 = (bf16[192,2048]{1,0:T(8,128)(2,1)S(1)}, bf16[192,2048]{1,0:T(8,128)(2,1)}, u32[]{:S(2)}) copy-start(bf16[192,2048]{1,0:T(8,128)(2,1)} %param.15) | copy-start | bytes 2359300
  231.1 9.7 %copy-start.3 = (f32[2048]{0:T(1024)S(1)}, f32[2048]{0:T(1024)}, u32[]{:S(2)}) copy-start(f32[2048]{0:T(1024)} %param.22) | copy-start | bytes 24580
  232.7 152.0 %all-gather.10.cloned.1.call-start = ((), (), s32[]{:S(2)}) async-start(), calls=%async_computation.5 | async-start | bytes 12255232 | tf_op jit(solution)/shard_map/all_gather | solution.py:112
  233.3 293.7 %all-gather.12.cloned.1.call-start = ((), (), s32[]{:S(2)}) async-start(), calls=%async_computation.6 | async-start | bytes 12255232 | tf_op jit(solution)/shard_map/all_gather | solution.py:117
  233.9 475.9 %all-gather.14.cloned.1.call-start = ((), (), s32[]{:S(2)}) async-start(), calls=%async_computation.7 | async-start | bytes 12255232 | tf_op jit(solution)/shard_map/all_gather | solution.py:123
  234.4 495.9 %reduce-scatter.5.cloned.1.call-start = ((), (), s32[]{:S(2)}) async-start(), calls=%async_computation.8 | async-start | bytes 1179648 | tf_op jit(solution)/shard_map/reduce_scatter | solution.py:126
  393.1 337.3 %copy-start.1 = (bf16[96,2048]{1,0:T(8,128)(2,1)S(1)}, bf16[96,2048]{1,0:T(8,128)(2,1)}, u32[]{:S(2)}) copy-start(bf16[96,2048]{1,0:T(8,128)(2,1)} %reduce-scatter.3.cloned.1.call-done) | copy-start | bytes 1179652
Sparse Core Ops, SparseCore 0:
  10.1 70.5 all-gather.5
  83.5 66.3 all-gather.7
  232.8 6.6 reduce-scatter.2
  242.2 142.5 all-gather.9
  387.3 139.5 all-gather.11
  529.5 180.2 all-gather.13
  723.9 6.3 reduce-scatter.4
where the time goes:
time: 743 us; the launch traced here: 742 us
  waiting for transfers between devices  613 us (83%)
  matrix products  55.5 us (7%)
  other arithmetic  27.8 us (4%)
  local copies, waits for them, and re-layouts  26 us (3%)
  between operations  13.6 us (2%)
    all_gather x1, waiting for transfers between devices, local(): lax.all_gather(down_weight, 'sp', axis=1, tiled=True)  183 us
    all_gather x1, waiting for transfers between devices, local(): lax.all_gather(gate_weight, 'sp', axis=0, tiled=True)  140 us
    all_gather x1, waiting for transfers between devices, local(): lax.all_gather(up_weight, 'sp', axis=0, tiled=True)  134 us
    all_gather x1, waiting for transfers between devices, local(): key_rows = lax.all_gather(keys, 'sp', axis=0, tiled=True)  72.7 us
    all_gather x1, waiting for transfers between devices, local(): value_rows = lax.all_gather(values, 'sp', axis=0, tiled=True)  69.2 us
    convert_element_type x4, other arithmetic, update(): expo.astype(jnp.bfloat16)  17.4 us
    dot_general x4, matrix products, update(): jnp.einsum('qhcd,khcd->chqk', query_four, key_part, preferred_element_typ...  16.9 us
  transfers between devices with their start and end apart: 7, of which 7 were waited for; matrix products, arithmetic and copies ran while one was open for 1% of the time, Pallas kernels for 0%

commit v1 on v0

v1 whole, which is shorter than its diff:
```python
import functools

import jax
import jax.numpy as jnp
from jax import lax
from jax.experimental import pallas as pl
from jax.experimental.pallas import tpu as pltpu
from jax.sharding import Mesh, PartitionSpec as P

QK = 64
VD = 128
BF = jnp.bfloat16
F32 = jnp.float32


def attn_kernel(pos_ref, lam_ref, q_ref, k_ref, v_ref, gain_ref, o_ref, s_ref, *, groups, planes, rows):
    p_self = pos_ref[0]
    span = planes * rows
    lane = lax.broadcasted_iota(jnp.int32, (rows, 2 * QK), 1)
    row_id = lax.broadcasted_iota(jnp.int32, (rows, span), 0)
    col_id = lax.broadcasted_iota(jnp.int32, (rows, span), 1)
    mask_one = col_id <= row_id + p_self * rows
    mask = jnp.concatenate([mask_one, mask_one], axis=0)
    lam = lam_ref[0]
    for zq in range(groups):
        q = q_ref[zq] * jnp.asarray(QK**-0.5, BF)
        zero = jnp.zeros_like(q)
        q2 = jnp.concatenate([jnp.where(lane < QK, q, zero), jnp.where(lane < QK, zero, q)], axis=0)
        m = None
        for zk in range(zq + 1):
            kc = jnp.concatenate([k_ref[p, zk] for p in range(planes)], axis=0)
            s = lax.dot_general(q2, kc, (((1,), (1,)), ((), ())), preferred_element_type=F32)
            if zk == zq:
                s = jnp.where(mask, s, -1e30)
            s_ref[:, zk * span : (zk + 1) * span] = s
            mc = jnp.max(s, axis=-1, keepdims=True)
            m = mc if m is None else jnp.maximum(m, mc)
        acc = jnp.zeros((2 * rows, VD), F32)
        tot = jnp.zeros((2 * rows, 1), F32)
        for zk in range(zq + 1):
            e = jnp.exp(s_ref[:, zk * span : (zk + 1) * span] - m)
            tot = tot + jnp.sum(e, axis=-1, keepdims=True)
            vc = jnp.concatenate([v_ref[p, zk] for p in range(planes)], axis=0)
            acc = acc + jnp.dot(e.astype(BF), vc, preferred_element_type=F32)
        ratio = acc / tot
        mixed = ratio[:rows] - lam * ratio[rows:]
        scale = lax.rsqrt(jnp.mean(mixed * mixed, axis=-1, keepdims=True) + 1e-05)
        o_ref[zq] = (mixed * scale * gain_ref[...]).astype(BF)


def attention_split(queries, keys, values, lambdas, head_gain, groups, planes):
    rows = queries.shape[0]
    heads = lambdas.shape[0]

    def exchange(x):
        parts = x.reshape(rows, groups, VD).transpose(1, 0, 2)
        return parts

    qkv = jnp.stack([exchange(keys), exchange(values), exchange(queries)], axis=1)
    qkv = lax.all_to_all(qkv, "z", 0, 0, tiled=True)
    kv = lax.all_gather(jnp.stack([qkv[:, 0], qkv[:, 1]]), "p", axis=0, tiled=False)
    lam = lax.dynamic_slice_in_dim(lambdas, lax.axis_index("z"), 1, 0)
    pos = lax.axis_index("p").astype(jnp.int32).reshape(1)
    out = pl.pallas_call(
        functools.partial(attn_kernel, groups=groups, planes=planes, rows=rows),
        out_shape=jax.ShapeDtypeStruct((groups, rows, VD), BF),
        in_specs=[
            pl.BlockSpec(memory_space=pltpu.SMEM),
            pl.BlockSpec(memory_space=pltpu.SMEM),
            pl.BlockSpec(memory_space=pltpu.VMEM),
            pl.BlockSpec(memory_space=pltpu.VMEM),
            pl.BlockSpec(memory_space=pltpu.VMEM),
            pl.BlockSpec(memory_space=pltpu.VMEM),
        ],
        out_specs=pl.BlockSpec(memory_space=pltpu.VMEM),
        scratch_shapes=[pltpu.VMEM((2 * rows, groups * planes * rows), F32)],
        cost_estimate=pl.CostEstimate(
            flops=8 * rows * rows * groups * groups * planes * VD,
            transcendentals=rows * rows * groups * groups * planes,
            bytes_accessed=4 * rows * groups * planes * VD,
        ),
        compiler_params=pltpu.CompilerParams(vmem_limit_bytes=40 * 1024 * 1024),
        name="attn",
    )(pos, lam, qkv[:, 2], kv[:, 0], kv[:, 1], head_gain.reshape(1, VD))
    back = lax.all_to_all(out, "z", 0, 0, tiled=True)
    return back


def attention_plain(queries, keys, values, lambdas, head_gain):
    tok_rows = queries.shape[0]
    local_heads = lambdas.shape[0]
    offset = (lax.axis_index("z") * lax.axis_size("p") + lax.axis_index("p")) * tok_rows
    query_four = queries.reshape(tok_rows, local_heads, 2, QK)
    query_pos = offset + lax.iota(jnp.int32, tok_rows)
    key_rows = lax.all_gather(keys, ("z", "p"), axis=0, tiled=True)
    value_rows = lax.all_gather(values, ("z", "p"), axis=0, tiled=True)
    key_count = key_rows.shape[0]
    key_span = key_count
    while key_span > 1024 and key_span % 2 == 0:
        key_span = key_span // 2

    def one_span(span_index, state):
        run_max, run_sum, run_acc = state
        start = span_index * key_span
        key_part = lax.dynamic_slice_in_dim(key_rows, start, key_span, 0)
        key_part = key_part.reshape(key_span, local_heads, 2, QK)
        value_part = lax.dynamic_slice_in_dim(value_rows, start, key_span, 0)
        value_part = value_part.reshape(key_span, local_heads, VD)
        key_pos = start + lax.iota(jnp.int32, key_span)
        scores = jnp.einsum("qhcd,khcd->chqk", query_four, key_part, preferred_element_type=F32)
        causal = key_pos[None, :] <= query_pos[:, None]
        scores = jnp.where(causal, scores * QK**-0.5, -1e30)
        new_max = jnp.maximum(run_max, jnp.max(scores, axis=-1))
        expo = jnp.where(causal, jnp.exp(scores - new_max[..., None]), 0.0)
        factor = jnp.exp(run_max - new_max)
        new_sum = run_sum * factor + jnp.sum(expo, axis=-1)
        new_acc = run_acc * factor[..., None] + jnp.einsum(
            "chqk,khd->chqd", expo.astype(BF), value_part, preferred_element_type=F32
        )
        return new_max, new_sum, new_acc

    initial = (
        jnp.full((2, local_heads, tok_rows), -1e30, F32),
        jnp.zeros((2, local_heads, tok_rows), F32),
        jnp.zeros((2, local_heads, tok_rows, VD), F32),
    )
    _, final_sum, final_acc = lax.fori_loop(0, key_count // key_span, one_span, initial)
    ratio = final_acc / final_sum[..., None]
    mixed = ratio[0] - lambdas[:, None, None] * ratio[1]
    scale = lax.rsqrt(jnp.mean(mixed * mixed, axis=-1, keepdims=True) + 1e-05)
    return (mixed * scale * head_gain).astype(BF)


def local(
    resid,
    queries,
    keys,
    values,
    lambdas,
    head_gain,
    out_weight,
    norm_gain,
    gate_weight,
    up_weight,
    down_weight,
):
    groups = lax.axis_size("z")
    planes = lax.axis_size("p")
    tok_rows, width = resid.shape
    local_heads = lambdas.shape[0]
    own_rows = tok_rows // lax.axis_size("tp")
    z_self = lax.axis_index("z")

    if local_heads == groups:
        head_out = attention_split(queries, keys, values, lambdas, head_gain, groups, planes)
    else:
        head_out = attention_plain(queries, keys, values, lambdas, head_gain)

    units = gate_weight.shape[1]
    span = -(-units // (groups * 128)) * 128
    starts = [min(g * span, units - span) for g in range(groups)]
    first_unit = z_self * span - jnp.minimum(z_self * span, units - span)
    k_rows = gate_weight.shape[0]

    gate_up = jnp.stack(
        [jnp.stack([gate_weight[:, s : s + span], up_weight[:, s : s + span]]) for s in starts]
    )
    gate_up = lax.all_to_all(gate_up, "z", 0, 0, tiled=True)
    gate_all = lax.all_gather(gate_up[:, 0], "p", axis=0, tiled=False).reshape(width, span)
    up_all = lax.all_gather(gate_up[:, 1], "p", axis=0, tiled=False).reshape(width, span)
    down = jnp.stack([down_weight[s : s + span] for s in starts])
    down = lax.all_to_all(down, "z", 0, 0, tiled=True)
    down_all = lax.all_gather(down, "p", axis=0, tiled=False)

    out_three = out_weight.reshape(local_heads, VD, width)
    branch = lax.psum_scatter(
        jnp.einsum("hqd,hde->qe", head_out, out_three, preferred_element_type=F32).astype(BF),
        "tp",
        scatter_dimension=0,
        tiled=True,
    ).astype(F32)
    resid_own = lax.dynamic_slice_in_dim(resid, lax.axis_index("tp") * own_rows, own_rows, 0)
    first = resid_own.astype(F32) + branch
    normed = first * lax.rsqrt(jnp.mean(first * first, axis=-1, keepdims=True) + 1e-06) * norm_gain
    normed = normed.astype(BF).reshape(own_rows, groups, planes, k_rows).transpose(0, 2, 1, 3)
    normed_all = lax.all_gather(normed.reshape(own_rows, width), ("z", "tp"), axis=0, tiled=True)
    gate_act = jnp.dot(normed_all, gate_all, preferred_element_type=F32)
    up_act = jnp.dot(normed_all, up_all, preferred_element_type=F32)
    keep = lax.iota(jnp.int32, span) >= first_unit
    hidden = jnp.where(keep[None, :], jax.nn.silu(gate_act) * up_act, 0.0).astype(BF)
    terms = jnp.einsum("th,pzhd->tzpd", hidden, down_all, preferred_element_type=F32)
    terms = terms.astype(BF).reshape(-1, width)
    mixer = lax.psum_scatter(terms, ("z", "tp"), scatter_dimension=0, tiled=True).astype(F32)
    finished = (first + 0.5 * mixer).astype(BF)
    return lax.all_gather(finished, "tp", axis=0, tiled=True)


def solution(mesh):
    sp, tp = mesh.shape["sp"], mesh.shape["tp"]
    groups = 4 if sp % 4 == 0 else 1
    split = Mesh(mesh.devices.reshape(groups, sp // groups, tp), ("z", "p", "tp"))
    rows = ("z", "p")
    return jax.shard_map(
        local,
        mesh=split,
        in_specs=(
            P(rows, None),
            P(rows, "tp"),
            P(rows, "tp"),
            P(rows, "tp"),
            P("tp"),
            P(),
            P("tp", None),
            P(),
            P(rows, "tp"),
            P(rows, "tp"),
            P("tp", rows),
        ),
        out_specs=P(rows, None),
        check_vma=False,
    )
```

time: 743 us -> 369 us (0.50)
  waiting for transfers between devices: 613 us -> 231 us
  blocking collectives: 4.87 us -> 47.4 us
  matrix products: 55.5 us -> 22.2 us
  other arithmetic: 27.8 us -> 8.28 us
  starting transfers between devices: 0.23 us -> 9.38 us
    all_gather x5, waiting for transfers between devices: 599 us -> 152 us  [the longest x1 39.7 us: local(): lax.all_gather(normed.reshape(own_rows, width), ('z', 'tp'), axis=0, tile...]
    all_to_all x0 -> x2, blocking collectives: none -> 45 us  [the longest x1 22.8 us: local(): down = lax.all_to_all(down, 'z', 0, 0, tiled=True)]
    all_to_all x0 -> x2, waiting for transfers between devices: none -> 38 us  [the longest x1 33.3 us: local(): gate_up = lax.all_to_all(gate_up, 'z', 0, 0, tiled=True)]
    reduce_scatter x1, waiting for transfers between devices: 6.5 us -> 40.5 us  [local(): lax.psum_scatter(terms, ('z', 'tp'), scatter_dimension=0, tiled=True)]
    dot_general x11 -> x4, matrix products: 55.5 us -> 22.2 us  [the longest x1 7.34 us: local(): up_act = jnp.dot(normed_all, up_all, preferred_element_type=F32)]
    dynamic_slice x12 -> x1, local copies, waits for them, and re-layouts: 23.3 us -> 0.64 us  [attention_split(): lam = lax.dynamic_slice_in_dim(lambdas, lax.axis_index('z'), 1, 0)]
    convert_element_type x6 -> x2, other arithmetic: 19.7 us -> 3.07 us  [the longest x1 1.9 us: local(): normed.astype(BF).reshape(own_rows, groups, planes, k_rows)]
    reshape x0 -> x7, local copies, waits for them, and re-layouts: none -> 13.5 us  [the longest x1 6.15 us: local(): terms = terms.astype(BF).reshape(-1, width)]
  transfers between devices with their start and end apart: 7 -> 9, of which waited for: 7 -> 8; matrix products, arithmetic and copies ran while one was open for 1% -> 9% of each run, Pallas kernels for 0% -> 0%
where the time goes in v1:
time: 369 us; the launch traced here: 368 us
  waiting for transfers between devices  231 us (63%)
  blocking collectives  47.4 us (13%)
  local copies, waits for them, and re-layouts  29.6 us (8%)
  matrix products  22.2 us (6%)
  between operations  13.7 us (4%)
  starting transfers between devices  9.38 us (3%)
  other arithmetic  8.28 us (2%)
  Pallas kernels  6.87 us (2%)
    reduce_scatter x1, waiting for transfers between devices, local(): lax.psum_scatter(terms, ('z', 'tp'), scatter_dimension=0, tiled=True)  40.5 us
    all_gather x1, waiting for transfers between devices, local(): lax.all_gather(normed.reshape(own_rows, width), ('z', 'tp'), axis=0, tile...  39.7 us
    all_gather x1, waiting for transfers between devices, local(): down_all = lax.all_gather(down, 'p', axis=0, tiled=False)  38.2 us
    all_gather x1, waiting for transfers between devices, local(): lax.all_gather(gate_up[:, 1], 'p', axis=0, tiled=False).reshape(width, span)  37.6 us
    all_to_all x1, waiting for transfers between devices, local(): gate_up = lax.all_to_all(gate_up, 'z', 0, 0, tiled=True)  33.3 us
    all_gather x1, waiting for transfers between devices, attention_split(): lax.all_gather(jnp.stack([qkv[:, 0], qkv[:, 1]]), 'p', axis=0, tiled=False)  26.6 us
    all_to_all x1, blocking collectives, local(): down = lax.all_to_all(down, 'z', 0, 0, tiled=True)  22.8 us
    all_to_all x1, blocking collectives, attention_split(): qkv = lax.all_to_all(qkv, 'z', 0, 0, tiled=True)  22.2 us
  transfers between devices with their start and end apart: 9, of which 8 were waited for; matrix products, arithmetic and copies ran while one was open for 9% of the time, Pallas kernels for 0%

profile of v1, /device:TPU:0, one launch (start us, length us, event | category | flops | bytes accessed | tf_op | source)
XLA Modules:
  0.0 368.2 jit_solution(18385084440392391543)
XLA Ops:
  10.3 22.2 %all_to_all.20 = bf16[4,3,192,128]{3,2,1,0:T(8,128)(2,1)S(1)} all-to-all(bf16[4,3,192,128]{3,2,1,0:T(8,128)(2,1)S(1)} %copy.22), channel_id=1, replica_groups=mesh['z'=4,'p'=4,'tp'=2] {'z'}, dimensions={0} | all-to-all | bytes 1179648 | tf_op jit(solution)/shard_map/all_to_all | solution.py:60
  34.8 2.0 slice_bitcast_fusion.11
  36.8 26.6 %all-gather.12.cloned.1.call-done = bf16[8,4,192,128]{3,2,1,0:T(8,128)(2,1)} async-done(((bf16[2,4,192,128]{3,2,1,0:T(8,128)(2,1)}), bf16[8,4,192,128]{3,2,1,0:T(8,128)(2,1)}) %all-gather.12.cloned.1.call-update) | async-done | bytes 1572880 | tf_op jit(solution)/shard_map/all_gather | solution.py:61
  63.4 1.5 slice_bitcast_fusion
  64.9 6.9 %attn.1 = bf16[4,192,128]{2,1,0:T(8,128)(2,1)} custom-call(s32[1]{0:T(128)} %bitcast.pos_ref, f32[1]{0:T(128)} %dynamic_slice.7.lam_ref, bf16[4,192,128]{2,1,0:T(8,128)(2,1)S(1)} %get-tuple-element.22.q_ref, bf16[4,4,192,128]{3,2,1,0:T(8,128)(2,1)S(1)} %get-tuple-element.8.k_ref, bf16[4,4,192,128]{3,2,1,0:T(8,128)(2,1)S(1)} %get-tuple-element.7.v_ref, ...), custom_call_target="tpu_custom_call" | custom-call | flops 2415919104 | bytes 1572864 | tf_op jit(solution)/shard_map/attn/pallas_call | solution.py:64
  71.8 4.6 %all-to-all-start.1 = ((bf16[4,192,128]{2,1,0:T(8,128)(2,1)}), bf16[4,192,128]{2,1,0:T(8,128)(2,1)S(1)}, u32[]{:S(2)}, u32[]{:S(2)}) async-start(bf16[4,192,128]{2,1,0:T(8,128)(2,1)} %attn.1), calls=%async_computation.1 | async-start | bytes 393216 | tf_op jit(solution)/shard_map/all_to_all | solution.py:85
  79.0 4.7 %all-to-all-done.1 = bf16[4,192,128]{2,1,0:T(8,128)(2,1)S(1)} async-done(((bf16[4,192,128]{2,1,0:T(8,128)(2,1)}), bf16[4,192,128]{2,1,0:T(8,128)(2,1)S(1)}, u32[]{:S(2)}, u32[]{:S(2)}) %all-to-all-start.1) | async-done | bytes 196640 | tf_op jit(solution)/shard_map/all_to_all | solution.py:85
  83.7 4.4 %all-to-all-start.3 = ((bf16[4,2,128,768]{3,2,1,0:T(8,128)(2,1)}), bf16[4,2,128,768]{3,2,1,0:T(8,128)(2,1)}, u32[]{:S(2)}, u32[]{:S(2)}) async-start(bf16[4,2,128,768]{3,2,1,0:T(8,128)(2,1)} %pad_maximum_fusion), calls=%async_computation.4 | async-start | bytes 3145728 | tf_op jit(solution)/shard_map/all_to_all | solution.py:168
  89.7 33.3 %all-to-all-done.3 = bf16[4,2,128,768]{3,2,1,0:T(8,128)(2,1)} async-done(((bf16[4,2,128,768]{3,2,1,0:T(8,128)(2,1)}), bf16[4,2,128,768]{3,2,1,0:T(8,128)(2,1)}, u32[]{:S(2)}, u32[]{:S(2)}) %all-to-all-start.3) | async-done | bytes 1572896 | tf_op jit(solution)/shard_map/all_to_all | solution.py:168
  122.9 2.6 fusion.2
  126.9 1.9 multiply_convert_fusion
  131.0 2.1 reshape.53
  135.1 22.8 %all_to_all.21 = bf16[4,768,128]{2,1,0:T(8,128)(2,1)} all-to-all(bf16[4,768,128]{2,1,0:T(8,128)(2,1)S(1)} %pad_maximum_fusion.1), channel_id=1, replica_groups=mesh['z'=4,'p'=4,'tp'=2] {'z'}, dimensions={0} | all-to-all | bytes 1572864 | tf_op jit(solution)/shard_map/all_to_all | solution.py:172
  158.2 9.5 %all-gather.16.cloned.1.call-done = bf16[16,1,128,768]{3,2,1,0:T(8,128)(2,1)} async-done(((bf16[4,1,128,768]{3,2,1,0:T(8,128)(2,1)}), bf16[16,1,128,768]{3,2,1,0:T(8,128)(2,1)}) %all-gather.16.cloned.1.call-update) | async-done | bytes 3145744 | tf_op jit(solution)/shard_map/all_gather | solution.py:169
  167.7 39.7 %all-gather.10.cloned.1.call-done = bf16[768,2048]{1,0:T(8,128)(2,1)} async-done(((bf16[96,2048]{1,0:T(8,128)(2,1)}), bf16[768,2048]{1,0:T(8,128)(2,1)}) %all-gather.10.cloned.1.call-update) | async-done | bytes 3145744 | tf_op jit(solution)/shard_map/all_gather | solution.py:186
  207.5 6.8 %fusion.3 = f32[768,768]{1,0:T(8,128)} fusion(bf16[768,2048]{1,0:T(8,128)(2,1)} %all-gather.10.cloned.1.call-done, bf16[2048,768]{1,0:T(8,128)(2,1)} %bitcast.95), kind=kOutput, calls=%fused_computation.38 | convolution fusion | flops 2415919104 | bytes 8650752 | tf_op jit(solution)/shard_map/dot_general | solution.py:187
  214.3 37.6 %all-gather.18.cloned.1.call-done = bf16[16,1,128,768]{3,2,1,0:T(8,128)(2,1)} async-done(((bf16[4,1,128,768]{3,2,1,0:T(8,128)(2,1)}), bf16[16,1,128,768]{3,2,1,0:T(8,128)(2,1)}) %all-gather.18.cloned.1.call-update) | async-done | bytes 3145744 | tf_op jit(solution)/shard_map/all_gather | solution.py:170
  251.9 7.3 %fusion.1 = bf16[768,768,1,1]{1,0,3,2:T(8,128)(2,1)} fusion(bf16[768,2048]{1,0:T(8,128)(2,1)} %all-gather.10.cloned.1.call-done, bf16[2048,768]{1,0:T(8,128)(2,1)} %bitcast.96, f32[768,768]{1,0:T(8,128)} %fusion.3, pred[768]{0:T(1024)(128)(4,1)S(1)} %iota_compare_fusion), kind=kOutput, calls=%fused_computation.5 | convolution fusion | flops 2420047872 | bytes 9831168 | tf_op jit(solution)/shard_map/dot_general | solution.py:188
  259.3 38.2 %all-gather.14.cloned.1.call-done = bf16[16,768,128]{2,1,0:T(8,128)(2,1)} async-done(((bf16[4,768,128]{2,1,0:T(8,128)(2,1)}), bf16[16,768,128]{2,1,0:T(8,128)(2,1)}) %all-gather.14.cloned.1.call-update) | async-done | bytes 3145744 | tf_op jit(solution)/shard_map/all_gather | solution.py:173
  297.5 6.6 %convert_bitcast_fusion = bf16[768,4,4,128]{0,3,1,2:T(8,128)(2,1)} fusion(bf16[4,4,768,128]{3,2,1,0:T(8,128)(2,1)} %bitcast.97, bf16[768,768,1,1]{1,0,3,2:T(8,128)(2,1)} %fusion.1), kind=kOutput, calls=%fused_computation | convolution fusion | flops 2417491968 | bytes 7471104 | tf_op jit(solution)/shard_map/th,pzhd->tzpd/dot_general | solution.py:191
  304.1 6.2 %copy.29 = bf16[768,4,4,128]{3,2,1,0:T(4,128)(2,1)} copy(bf16[768,4,4,128]{0,3,1,2:T(8,128)(2,1)} %convert_bitcast_fusion) | data formatting | bytes 6291456 | tf_op jit(solution)/shard_map/convert_element_type | solution.py:192
  310.2 6.1 %reshape.56 = bf16[768,2048]{1,0:T(8,128)(2,1)} reshape(bf16[768,4,4,128]{3,2,1,0:T(4,128)(2,1)} %copy.29) | data formatting | bytes 6291456 | tf_op jit(solution)/shard_map/reshape | solution.py:192
  316.4 40.5 %reduce-scatter.5.cloned.1.call-done = bf16[96,2048]{1,0:T(8,128)(2,1)} async-done(((bf16[768,2048]{1,0:T(8,128)(2,1)}), bf16[96,2048]{1,0:T(8,128)(2,1)}) %reduce-scatter.5.cloned.1.call-update) | async-done | bytes 393232 | tf_op jit(solution)/shard_map/reduce_scatter | solution.py:193
  358.1 2.4 all_gather.31
  (53 shorter events, 18.0 us)
Async XLA Ops:
  6.5 81.6 %copy-start = (bf16[512,2048]{1,0:T(8,128)(2,1)S(1)}, bf16[512,2048]{1,0:T(8,128)(2,1)}, u32[]{:S(2)}) copy-start(bf16[512,2048]{1,0:T(8,128)(2,1)} %param.17) | copy-start | bytes 6291460
  6.5 56.9 %all-gather.12.cloned.1.call-start = ((), (), s32[]{:S(2)}) async-start(), calls=%async_computation.9 | async-start | bytes 1966080 | tf_op jit(solution)/shard_map/all_gather | solution.py:61
  10.1 23.2 %copy-start.7 = (f32[4]{0:T(128)S(1)}, f32[4]{0:T(128)}, u32[]{:S(2)}) copy-start(f32[4]{0:T(128)} %param.15) | copy-start | bytes 52
  10.1 23.8 %copy-start.4 = (bf16[128,2816]{1,0:T(8,128)(2,1)S(1)}, bf16[128,2816]{1,0:T(8,128)(2,1)}, u32[]{:S(2)}) copy-start(bf16[128,2816]{1,0:T(8,128)(2,1)} %param.19) | copy-start | bytes 2162692
  34.8 30.1 %copy-start.1 = (f32[128]{0:T(128)S(1)}, f32[128]{0:T(128)}, u32[]{:S(2)}) copy-start(f32[128]{0:T(128)} %param.16) | copy-start | bytes 1540
  64.9 11.5 %copy-start.5 = (bf16[1,128,768]{2,1,0:T(8,128)(2,1)S(1)}, bf16[1,128,768]{2,1,0:T(8,128)(2,1)}, u32[]{:S(2)}) copy-start(bf16[1,128,768]{2,1,0:T(8,128)(2,1)} %get-tuple-element.9) | copy-start | bytes 589828
  71.8 11.9 %all-to-all-start.1 = ((bf16[4,192,128]{2,1,0:T(8,128)(2,1)}), bf16[4,192,128]{2,1,0:T(8,128)(2,1)S(1)}, u32[]{:S(2)}, u32[]{:S(2)}) async-start(bf16[4,192,128]{2,1,0:T(8,128)(2,1)} %attn.1), calls=%async_computation.1 | async-start | bytes 393216 | tf_op jit(solution)/shard_map/all_to_all | solution.py:85
  83.7 39.3 %all-to-all-start.3 = ((bf16[4,2,128,768]{3,2,1,0:T(8,128)(2,1)}), bf16[4,2,128,768]{3,2,1,0:T(8,128)(2,1)}, u32[]{:S(2)}, u32[]{:S(2)}) async-start(bf16[4,2,128,768]{3,2,1,0:T(8,128)(2,1)} %pad_maximum_fusion), calls=%async_computation.4 | async-start | bytes 3145728 | tf_op jit(solution)/shard_map/all_to_all | solution.py:168
  88.0 37.6 %reduce-scatter.3.cloned.1.call-start = ((), (), s32[]{:S(2)}) async-start(), calls=%async_computation.6 | async-start | bytes 1179648 | tf_op jit(solution)/shard_map/reduce_scatter | solution.py:176
  89.6 36.1 %copy-start.3 = (bf16[192,2048]{1,0:T(8,128)(2,1)S(1)}, bf16[192,2048]{1,0:T(8,128)(2,1)}, u32[]{:S(2)}) copy-start(bf16[192,2048]{1,0:T(8,128)(2,1)} %param.11) | copy-start | bytes 2359300
  89.6 37.3 %copy-start.6 = (f32[2048]{0:T(1024)S(1)}, f32[2048]{0:T(1024)}, u32[]{:S(2)}) copy-start(f32[2048]{0:T(1024)} %param.18) | copy-start | bytes 24580
  89.6 78.1 %all-gather.16.cloned.1.call-start = ((), (), s32[]{:S(2)}) async-start(), calls=%async_computation.11 | async-start | bytes 3932160 | tf_op jit(solution)/shard_map/all_gather | solution.py:169
  125.6 81.9 %all-gather.10.cloned.1.call-start = ((), (), s32[]{:S(2)}) async-start(), calls=%async_computation.7 | async-start | bytes 3538944 | tf_op jit(solution)/shard_map/all_gather | solution.py:186
  133.1 118.8 %all-gather.18.cloned.1.call-start = ((), (), s32[]{:S(2)}) async-start(), calls=%async_computation.12 | async-start | bytes 3932160 | tf_op jit(solution)/shard_map/all_gather | solution.py:170
  133.7 163.8 %all-gather.14.cloned.1.call-start = ((), (), s32[]{:S(2)}) async-start(), calls=%async_computation.10 | async-start | bytes 3932160 | tf_op jit(solution)/shard_map/all_gather | solution.py:173
  158.0 199.0 %reduce-scatter.5.cloned.1.call-start = ((), (), s32[]{:S(2)}) async-start(), calls=%async_computation.8 | async-start | bytes 3538944 | tf_op jit(solution)/shard_map/reduce_scatter | solution.py:193
  316.4 40.6 %copy-start.2 = (bf16[96,2048]{1,0:T(8,128)(2,1)S(1)}, bf16[96,2048]{1,0:T(8,128)(2,1)}, u32[]{:S(2)}) copy-start(bf16[96,2048]{1,0:T(8,128)(2,1)} %reduce-scatter.3.cloned.1.call-done) | copy-start | bytes 1179652
Sparse Core Ops, SparseCore 0:
  33.4 29.9 all-gather.11
  91.1 8.5 reduce-scatter.2
  125.7 41.9 all-gather.15
  169.2 38.2 all-gather.9
  209.1 42.7 all-gather.17
  253.6 43.8 all-gather.13
  316.5 40.3 reduce-scatter.4

commit v2 on v1

--- a/solution.py
+++ b/solution.py
@@ -7,6 +7,7 @@
 from jax.experimental.pallas import tpu as pltpu
 from jax.sharding import Mesh, PartitionSpec as P
 
+
 QK = 64
 VD = 128
 BF = jnp.bfloat16
@@ -14,7 +15,8 @@
 
 
 def attn_kernel(pos_ref, lam_ref, q_ref, k_ref, v_ref, gain_ref, o_ref, s_ref, *, groups, planes, rows):
-    p_self = pos_ref[0]
+    z_self = pos_ref[0]
+    p_self = pos_ref[1]
     span = planes * rows
     lane = lax.broadcasted_iota(jnp.int32, (rows, 2 * QK), 1)
     row_id = lax.broadcasted_iota(jnp.int32, (rows, span), 0)
@@ -23,12 +25,12 @@
     mask = jnp.concatenate([mask_one, mask_one], axis=0)
     lam = lam_ref[0]
     for zq in range(groups):
-        q = q_ref[zq] * jnp.asarray(QK**-0.5, BF)
+        q = q_ref[z_self ^ zq] * jnp.asarray(QK**-0.5, BF)
         zero = jnp.zeros_like(q)
         q2 = jnp.concatenate([jnp.where(lane < QK, q, zero), jnp.where(lane < QK, zero, q)], axis=0)
         m = None
         for zk in range(zq + 1):
-            kc = jnp.concatenate([k_ref[p, zk] for p in range(planes)], axis=0)
+            kc = jnp.concatenate([k_ref[p_self ^ p, z_self ^ zk] for p in range(planes)], axis=0)
             s = lax.dot_general(q2, kc, (((1,), (1,)), ((), ())), preferred_element_type=F32)
             if zk == zq:
                 s = jnp.where(mask, s, -1e30)
@@ -40,50 +42,156 @@
         for zk in range(zq + 1):
             e = jnp.exp(s_ref[:, zk * span : (zk + 1) * span] - m)
             tot = tot + jnp.sum(e, axis=-1, keepdims=True)
-            vc = jnp.concatenate([v_ref[p, zk] for p in range(planes)], axis=0)
+            vc = jnp.concatenate([v_ref[p_self ^ p, z_self ^ zk] for p in range(planes)], axis=0)
             acc = acc + jnp.dot(e.astype(BF), vc, preferred_element_type=F32)
         ratio = acc / tot
         mixed = ratio[:rows] - lam * ratio[rows:]
         scale = lax.rsqrt(jnp.mean(mixed * mixed, axis=-1, keepdims=True) + 1e-05)
-        o_ref[zq] = (mixed * scale * gain_ref[...]).astype(BF)
-
-
-def attention_split(queries, keys, values, lambdas, head_gain, groups, planes):
-    rows = queries.shape[0]
-    heads = lambdas.shape[0]
-
-    def exchange(x):
-        parts = x.reshape(rows, groups, VD).transpose(1, 0, 2)
-        return parts
-
-    qkv = jnp.stack([exchange(keys), exchange(values), exchange(queries)], axis=1)
-    qkv = lax.all_to_all(qkv, "z", 0, 0, tiled=True)
-    kv = lax.all_gather(jnp.stack([qkv[:, 0], qkv[:, 1]]), "p", axis=0, tiled=False)
-    lam = lax.dynamic_slice_in_dim(lambdas, lax.axis_index("z"), 1, 0)
-    pos = lax.axis_index("p").astype(jnp.int32).reshape(1)
+        o_ref[z_self ^ zq] = (mixed * scale * gain_ref[...]).astype(BF)
+
+
+def mixer_kernel(pos_ref, x_ref, *refs, rows):
+    gates, ups, downs = refs[0:4], refs[4:8], refs[8:12]
+    o_ref = refs[12]
+    z_self, p_self, first_unit = pos_ref[0], pos_ref[1], pos_ref[2]
+    block = downs[0].shape[2]
+    span = gates[0].shape[1]
+
+    def lanes(i, j):
+        return pl.ds(pl.multiple_of(((z_self ^ j) * 4 + (p_self ^ i)) * block, block), block)
+
+    def step(n, carry):
+        at = pl.ds(pl.multiple_of(n * rows, rows), rows)
+        gate = jnp.zeros((rows, span), F32)
+        up = jnp.zeros((rows, span), F32)
+        for i in range(4):
+            x = jnp.concatenate([x_ref[at, lanes(i, j)] for j in range(4)], axis=1)
+            gate = gate + jnp.dot(x, gates[i][...], preferred_element_type=F32)
+            up = up + jnp.dot(x, ups[i][...], preferred_element_type=F32)
+        hidden = gate / (1.0 + jnp.exp(-gate)) * up
+        keep = lax.broadcasted_iota(jnp.int32, (rows, span), 1) >= first_unit
+        hidden = jnp.where(keep, hidden, 0.0).astype(BF)
+        for i in range(4):
+            down = jnp.concatenate([downs[i][j] for j in range(4)], axis=1)
+            out = jnp.dot(hidden, down, preferred_element_type=F32).astype(BF)
+            for j in range(4):
+                o_ref[at, lanes(i, j)] = out[:, j * block : (j + 1) * block]
+        return carry
+
+    lax.fori_loop(0, x_ref.shape[0] // rows, step, 0)
+
+
+def swap(x, axis, bit):
+    size = lax.axis_size(axis)
+    return lax.ppermute(x, axis, [(i, i ^ bit) for i in range(size)])
+
+
+def plane_gather(x, first_bit):
+    one, two = swap(x, "p", 1), swap(x, "p", 2)
+    diag = swap(one, "p", 2) if first_bit == 1 else swap(two, "p", 1)
+    return [x, one, two, diag]
+
+
+def z_exchange(part):
+    z_self = lax.axis_index("z")
+    sends = [part(z_self ^ j) for j in range(1, 4)]
+    got = [swap(x, "z", j + 1) for j, x in enumerate(sends)]
+    return jnp.stack([part(z_self)] + got)
+
+
+def fast_local(
+    resid,
+    queries,
+    keys,
+    values,
+    lambdas,
+    head_gain,
+    out_weight,
+    norm_gain,
+    gate_weight,
+    up_weight,
+    down_weight,
+):
+    tok_rows, width = resid.shape
+    own_rows = tok_rows // lax.axis_size("tp")
+    z_self = lax.axis_index("z").astype(jnp.int32)
+    p_self = lax.axis_index("p").astype(jnp.int32)
+
+    def head(x):
+        return lambda g: lax.dynamic_slice_in_dim(x, g * VD, VD, 1)
+
+    qkv = z_exchange(lambda g: jnp.stack([head(x)(g) for x in (keys, values, queries)]))
+    key_all = jnp.stack(plane_gather(qkv[:, 0], 1))
+    value_all = jnp.stack(plane_gather(qkv[:, 1], 2))
+
+    units = gate_weight.shape[1]
+    span = -(-units // 512) * 128
+
+    def start(g):
+        return jnp.minimum(g * span, units - span)
+
+    gate_mine = z_exchange(lambda g: lax.dynamic_slice_in_dim(gate_weight, start(g), span, 1))
+    up_mine = z_exchange(lambda g: lax.dynamic_slice_in_dim(up_weight, start(g), span, 1))
+    down_mine = z_exchange(lambda g: lax.dynamic_slice_in_dim(down_weight, start(g), span, 0))
+    gates = plane_gather(gate_mine.reshape(-1, span), 1)
+    ups = plane_gather(up_mine.reshape(-1, span), 2)
+    half = span // 2
+    low = plane_gather(down_mine[:, :half], 1)
+    high = plane_gather(down_mine[:, half:], 2)
+    downs = [jnp.concatenate(pair, axis=1) for pair in zip(low, high)]
+
+    lam = lax.dynamic_slice_in_dim(lambdas, z_self, 1, 0)
+    smem = pl.BlockSpec(memory_space=pltpu.SMEM)
+    vmem = pl.BlockSpec(memory_space=pltpu.VMEM)
+    keys_total = 16 * tok_rows
     out = pl.pallas_call(
-        functools.partial(attn_kernel, groups=groups, planes=planes, rows=rows),
-        out_shape=jax.ShapeDtypeStruct((groups, rows, VD), BF),
-        in_specs=[
-            pl.BlockSpec(memory_space=pltpu.SMEM),
-            pl.BlockSpec(memory_space=pltpu.SMEM),
-            pl.BlockSpec(memory_space=pltpu.VMEM),
-            pl.BlockSpec(memory_space=pltpu.VMEM),
-            pl.BlockSpec(memory_space=pltpu.VMEM),
-            pl.BlockSpec(memory_space=pltpu.VMEM),
-        ],
-        out_specs=pl.BlockSpec(memory_space=pltpu.VMEM),
-        scratch_shapes=[pltpu.VMEM((2 * rows, groups * planes * rows), F32)],
+        functools.partial(attn_kernel, groups=4, planes=4, rows=tok_rows),
+        out_shape=jax.ShapeDtypeStruct((4, tok_rows, VD), BF),
+        in_specs=[smem, smem, vmem, vmem, vmem, vmem],
+        out_specs=vmem,
+        scratch_shapes=[pltpu.VMEM((2 * tok_rows, keys_total), F32)],
         cost_estimate=pl.CostEstimate(
-            flops=8 * rows * rows * groups * groups * planes * VD,
-            transcendentals=rows * rows * groups * groups * planes,
-            bytes_accessed=4 * rows * groups * planes * VD,
+            flops=3 * tok_rows * keys_total * 4 * VD * 2,
+            transcendentals=5 * tok_rows * keys_total,
+            bytes_accessed=4 * keys_total * VD,
         ),
         compiler_params=pltpu.CompilerParams(vmem_limit_bytes=40 * 1024 * 1024),
         name="attn",
-    )(pos, lam, qkv[:, 2], kv[:, 0], kv[:, 1], head_gain.reshape(1, VD))
-    back = lax.all_to_all(out, "z", 0, 0, tiled=True)
-    return back
+    )(jnp.stack([z_self, p_self]), lam, qkv[:, 2], key_all, value_all, head_gain.reshape(1, VD))
+    back = z_exchange(lambda g: lax.dynamic_index_in_dim(out, g ^ z_self, 0, keepdims=False))
+    head_out = jnp.concatenate(
+        [lax.dynamic_index_in_dim(back, z_self ^ h, 0, keepdims=False) for h in range(4)], axis=1
+    )
+    projected = jnp.dot(head_out, out_weight, preferred_element_type=F32).astype(BF)
+    branch = lax.psum_scatter(
+        projected,
+        "tp",
+        scatter_dimension=0,
+        tiled=True,
+    ).astype(F32)
+    resid_own = lax.dynamic_slice_in_dim(resid, lax.axis_index("tp") * own_rows, own_rows, 0)
+    first = resid_own.astype(F32) + branch
+    normed = first * lax.rsqrt(jnp.mean(first * first, axis=-1, keepdims=True) + 1e-06) * norm_gain
+    normed_all = lax.all_gather(normed.astype(BF), ("z", "tp"), axis=0, tiled=True)
+    first_unit = z_self * span - start(z_self)
+    tokens = normed_all.shape[0]
+    step = 256 if tokens % 256 == 0 else tokens
+    terms = pl.pallas_call(
+        functools.partial(mixer_kernel, rows=step),
+        out_shape=jax.ShapeDtypeStruct((tokens, width), BF),
+        in_specs=[smem] + [vmem] * 13,
+        out_specs=vmem,
+        cost_estimate=pl.CostEstimate(
+            flops=6 * tokens * width * span,
+            transcendentals=tokens * span,
+            bytes_accessed=6 * width * span + 4 * tokens * width,
+        ),
+        compiler_params=pltpu.CompilerParams(vmem_limit_bytes=50 * 1024 * 1024),
+        name="mixer",
+    )(jnp.stack([z_self, p_self, first_unit]), normed_all, *gates, *ups, *downs)
+    mixer = lax.psum_scatter(terms, ("z", "tp"), scatter_dimension=0, tiled=True).astype(F32)
+    finished = (first + 0.5 * mixer).astype(BF)
+    return lax.all_gather(finished, "tp", axis=0, tiled=True)
 
 
 def attention_plain(queries, keys, values, lambdas, head_gain):
@@ -151,10 +259,7 @@
     own_rows = tok_rows // lax.axis_size("tp")
     z_self = lax.axis_index("z")
 
-    if local_heads == groups:
-        head_out = attention_split(queries, keys, values, lambdas, head_gain, groups, planes)
-    else:
-        head_out = attention_plain(queries, keys, values, lambdas, head_gain)
+    head_out = attention_plain(queries, keys, values, lambdas, head_gain)
 
     units = gate_weight.shape[1]
     span = -(-units // (groups * 128)) * 128
@@ -200,8 +305,15 @@
     groups = 4 if sp % 4 == 0 else 1
     split = Mesh(mesh.devices.reshape(groups, sp // groups, tp), ("z", "p", "tp"))
     rows = ("z", "p")
+
+    def chosen(resid, queries, keys, values, lambdas, *rest):
+        four = groups == 4 and sp // groups == 4 and lambdas.shape[0] == 4
+        if four and rest[-1].shape[1] == 128:
+            return fast_local(resid, queries, keys, values, lambdas, *rest)
+        return local(resid, queries, keys, values, lambdas, *rest)
+
     return jax.shard_map(
-        local,
+        chosen,
         mesh=split,
         in_specs=(
             P(rows, None),

time: 369 us -> 303 us (0.82)
  starting transfers between devices: 9.38 us -> 63.7 us
  waiting for transfers between devices: 231 us -> 181 us
  blocking collectives: 47.4 us -> 2.37 us
  local copies, waits for them, and re-layouts: 29.6 us -> 7.08 us
  matrix products: 22.2 us -> 1.47 us
  Pallas kernels: 6.87 us -> 21.4 us
  other arithmetic: 8.28 us -> 12 us
    all_gather x5 -> x1, waiting for transfers between devices: 152 us -> 0.02 us  [fast_local(): lax.all_gather(normed.astype(BF), ('z', 'tp'), axis=0, tiled=True)]
    ppermute x0 -> x33, waiting for transfers between devices: none -> 133 us  [swap(): return lax.ppermute(x, axis, [(i, i ^ bit) for i in range(size)])]
    ppermute x0 -> x33, starting transfers between devices: none -> 63.5 us  [swap(): return lax.ppermute(x, axis, [(i, i ^ bit) for i in range(size)])]
    all_to_all x2 -> x0, blocking collectives: 45 us -> none  [the longest x1 22.8 us: local(): down = lax.all_to_all(down, 'z', 0, 0, tiled=True)]
    all_to_all x2 -> x0, waiting for transfers between devices: 38 us -> none  [the longest x1 33.3 us: local(): gate_up = lax.all_to_all(gate_up, 'z', 0, 0, tiled=True)]
    dot_general x4 -> x1, matrix products: 22.2 us -> 1.47 us  [fast_local(): jnp.dot(head_out, out_weight, preferred_element_type=F32).astype(BF)]
    pallas_call x1 -> x2, Pallas kernels: 6.87 us -> 21.4 us  [the longest x1 14.6 us: fast_local(): pl.pallas_call(functools.partial(mixer_kernel, rows=step), out_shape=jax....]
    reshape x7 -> x0, local copies, waits for them, and re-layouts: 13.5 us -> none  [the longest x1 6.15 us: local(): terms = terms.astype(BF).reshape(-1, width)]
  transfers between devices with their start and end apart: 9 -> 36, of which waited for: 8 -> 16; matrix products, arithmetic and copies ran while one was open for 9% -> 3% of each run, Pallas kernels for 0% -> 0%
where the time goes in v2:
time: 303 us; the launch traced here: 302 us
  waiting for transfers between devices  181 us (60%)
  starting transfers between devices  63.7 us (21%)
  Pallas kernels  21.4 us (7%)
  between operations  13.4 us (4%)
  other arithmetic  12 us (4%)
  local copies, waits for them, and re-layouts  7.08 us (2%)
    ppermute x33, waiting for transfers between devices, swap(): return lax.ppermute(x, axis, [(i, i ^ bit) for i in range(size)])  133 us
    ppermute x33, starting transfers between devices, swap(): return lax.ppermute(x, axis, [(i, i ^ bit) for i in range(size)])  63.5 us
    reduce_scatter x1, waiting for transfers between devices, fast_local(): lax.psum_scatter(terms, ('z', 'tp'), scatter_dimension=0, tiled=True)  39.7 us
    pallas_call x1, Pallas kernels, fast_local(): pl.pallas_call(functools.partial(mixer_kernel, rows=step), out_shape=jax....  14.6 us
    reduce_scatter x1, waiting for transfers between devices, fast_local(): lax.psum_scatter(projected, 'tp', scatter_dimension=0, tiled=True)  7.78 us
    pallas_call x1, Pallas kernels, fast_local(): pl.pallas_call(functools.partial(attn_kernel, groups=4, planes=4, rows=to...  6.84 us
  transfers between devices with their start and end apart: 36, of which 16 were waited for; matrix products, arithmetic and copies ran while one was open for 3% of the time, Pallas kernels for 0%

profile of v2, /device:TPU:0, one launch (start us, length us, event | category | flops | bytes accessed | tf_op | source)
XLA Modules:
  0.0 302.3 jit_solution(6413150311987616278)
XLA Ops:
  8.6 4.1 %collective-permute-start.1 = (bf16[3,192,128]{2,1,0:T(8,128)(2,1)S(1)}, bf16[3,192,128]{2,1,0:T(8,128)(2,1)S(1)}, u32[]{:S(2)}, u32[]{:S(2)}) collective-permute-start(bf16[3,192,128]{2,1,0:T(8,128)(2,1)S(1)} %pad_maximum_fusion.11), channel_id=1, source_target_pairs={{0,16},{8,24},{16,0},{24,8},{1,17},{9,25},{17,1},{25,9},{2,18},{10... | collective-permute-start | bytes 442376 | tf_op jit(solution)/shard_map/ppermute | solution.py:86
  14.6 9.3 %collective-permute-done.1 = bf16[3,192,128]{2,1,0:T(8,128)(2,1)S(1)} collective-permute-done((bf16[3,192,128]{2,1,0:T(8,128)(2,1)S(1)}, bf16[3,192,128]{2,1,0:T(8,128)(2,1)S(1)}, u32[]{:S(2)}, u32[]{:S(2)}) %collective-permute-start.1) | collective-permute-done | bytes 147488 | tf_op jit(solution)/shard_map/ppermute | solution.py:86
  28.4 2.1 collective-permute-done.3
  34.7 2.7 collective-permute-done.4
  37.4 2.1 collective-permute-done.5
  40.8 6.8 %attn.1 = bf16[4,192,128]{2,1,0:T(8,128)(2,1)S(1)} custom-call(s32[2]{0:T(128)S(1)} %pad_add_fusion.pos_ref, f32[1]{0:T(128)} %dynamic_slice.104.lam_ref, bf16[4,192,128]{2,1,0:T(8,128)(2,1)S(1)} %get-tuple-element.23.q_ref, bf16[4,4,192,128]{3,2,1,0:T(8,128)(2,1)S(1)} %pad_maximum_fusion.k_ref, bf16[4,4,192,128]{3,2,1,0:T(8,128)(2,1)S(1)} %pad_maximum_fusion.1.v_ref, ...), custom_call_target="tpu_custom_call" | custom-call | flops 1811939328 | bytes 1572864 | tf_op jit(solution)/shard_map/attn/pallas_call | solution.py:147
  47.7 4.6 %collective-permute-start.11 = (bf16[192,128]{1,0:T(8,128)(2,1)S(1)}, bf16[192,128]{1,0:T(8,128)(2,1)S(1)}, u32[]{:S(2)}, u32[]{:S(2)}) collective-permute-start(bf16[192,128]{1,0:T(8,128)(2,1)S(1)} %get-tuple-element.29), channel_id=1, source_target_pairs={{0,24},{8,16},{16,8},{24,0},{1,25},{9,17},{17,9},{25,1},{2,26},{10... | collective-permute-start | bytes 147464 | tf_op jit(solution)/shard_map/ppermute | solution.py:86
  52.3 2.8 collective-permute-start.10
  55.6 2.2 collective-permute-done.10
  60.8 7.8 %reduce-scatter.3.cloned.1.call-done = bf16[96,2048]{1,0:T(8,128)(2,1)} async-done(((bf16[192,2048]{1,0:T(8,128)(2,1)}), bf16[96,2048]{1,0:T(8,128)(2,1)}) %reduce-scatter.3.cloned.1.call-update) | async-done | bytes 393232 | tf_op jit(solution)/shard_map/reduce_scatter | solution.py:166
  75.3 2.4 collective-permute-start.26
  80.9 6.8 %collective-permute-start.14 = (bf16[128,768]{1,0:T(8,128)(2,1)S(1)}, bf16[128,768]{1,0:T(8,128)(2,1)S(1)}, u32[]{:S(2)}, u32[]{:S(2)}) collective-permute-start(bf16[128,768]{1,0:T(8,128)(2,1)S(1)} %get-tuple-element.17), channel_id=1, source_target_pairs={{0,24},{8,16},{16,8},{24,0},{1,25},{9,17},{17,9},{25,1},{2,26},{10... | collective-permute-start | bytes 589832 | tf_op jit(solution)/shard_map/ppermute | solution.py:86
  87.7 2.6 collective-permute-done.26
  90.2 9.9 %collective-permute-start.13 = (bf16[128,768]{1,0:T(8,128)(2,1)S(1)}, bf16[128,768]{1,0:T(8,128)(2,1)S(1)}, u32[]{:S(2)}, u32[]{:S(2)}) collective-permute-start(bf16[128,768]{1,0:T(8,128)(2,1)S(1)} %get-tuple-element.18), channel_id=1, source_target_pairs={{0,16},{8,24},{16,0},{24,8},{1,17},{9,25},{17,1},{25,9},{2,18},{10... | collective-permute-start | bytes 589832 | tf_op jit(solution)/shard_map/ppermute | solution.py:86
  100.1 6.0 %collective-permute-done.25 = bf16[768,128]{1,0:T(8,128)(2,1)S(1)} collective-permute-done((bf16[768,128]{1,0:T(8,128)(2,1)S(1)}, bf16[768,128]{1,0:T(8,128)(2,1)S(1)}, u32[]{:S(2)}, u32[]{:S(2)}) %collective-permute-start.25) | collective-permute-done | bytes 196640 | tf_op jit(solution)/shard_map/ppermute | solution.py:86
  106.1 6.3 %collective-permute-start.20 = (bf16[128,768]{1,0:T(8,128)(2,1)S(1)}, bf16[128,768]{1,0:T(8,128)(2,1)S(1)}, u32[]{:S(2)}, u32[]{:S(2)}) collective-permute-start(bf16[128,768]{1,0:T(8,128)(2,1)S(1)} %get-tuple-element.13), channel_id=1, source_target_pairs={{0,24},{8,16},{16,8},{24,0},{1,25},{9,17},{17,9},{25,1},{2,26},{10... | collective-permute-start | bytes 589832 | tf_op jit(solution)/shard_map/ppermute | solution.py:86
  112.7 25.6 %collective-permute-done.20 = bf16[128,768]{1,0:T(8,128)(2,1)S(1)} collective-permute-done((bf16[128,768]{1,0:T(8,128)(2,1)S(1)}, bf16[128,768]{1,0:T(8,128)(2,1)S(1)}, u32[]{:S(2)}, u32[]{:S(2)}) %collective-permute-start.20) | collective-permute-done | bytes 196640 | tf_op jit(solution)/shard_map/ppermute | solution.py:86
  139.8 14.7 %collective-permute-done.19 = bf16[128,768]{1,0:T(8,128)(2,1)S(1)} collective-permute-done((bf16[128,768]{1,0:T(8,128)(2,1)S(1)}, bf16[128,768]{1,0:T(8,128)(2,1)S(1)}, u32[]{:S(2)}, u32[]{:S(2)}) %collective-permute-start.19) | collective-permute-done | bytes 196640 | tf_op jit(solution)/shard_map/ppermute | solution.py:86
  161.2 25.0 %collective-permute-done.27 = bf16[4,384,128]{2,1,0:T(8,128)(2,1)S(1)} collective-permute-done((bf16[4,384,128]{2,1,0:T(8,128)(2,1)S(1)}, bf16[4,384,128]{2,1,0:T(8,128)(2,1)S(1)}, u32[]{:S(2)}, u32[]{:S(2)}) %collective-permute-start.27) | collective-permute-done | bytes 393248 | tf_op jit(solution)/shard_map/ppermute | solution.py:86
  188.2 6.4 %collective-permute-done.28 = bf16[4,384,128]{2,1,0:T(8,128)(2,1)S(1)} collective-permute-done((bf16[4,384,128]{2,1,0:T(8,128)(2,1)S(1)}, bf16[4,384,128]{2,1,0:T(8,128)(2,1)S(1)}, u32[]{:S(2)}, u32[]{:S(2)}) %collective-permute-start.28) | collective-permute-done | bytes 393248 | tf_op jit(solution)/shard_map/ppermute | solution.py:86
  202.6 32.5 %collective-permute-done.32 = bf16[4,384,128]{2,1,0:T(8,128)(2,1)} collective-permute-done((bf16[4,384,128]{2,1,0:T(8,128)(2,1)}, bf16[4,384,128]{2,1,0:T(8,128)(2,1)}, u32[]{:S(2)}, u32[]{:S(2)}) %collective-permute-start.32) | collective-permute-done | bytes 393248 | tf_op jit(solution)/shard_map/ppermute | solution.py:86
  237.1 14.6 %mixer.1 = bf16[768,2048]{1,0:T(8,128)(2,1)} custom-call(s32[3]{0:T(128)S(1)} %pad_add_fusion.1.pos_ref, bf16[768,2048]{1,0:T(8,128)(2,1)} %all-gather.2.cloned.1.call-done.x_ref, bf16[512,768]{1,0:T(8,128)(2,1)} %bitcast.45.refs_0_, bf16[512,768]{1,0:T(8,128)(2,1)} %collective-permute-done.15.refs_1_, bf16[512,768]{1,0:T(8,128)(2,1)} %collective-permute-done.16.refs_2_, ...), custom_call_target="tpu_custom_call" | custom-call | flops 7247757312 | bytes 15728640 | tf_op jit(solution)/shard_map/mixer/pallas_call | solution.py:179
  251.7 39.7 %reduce-scatter.5.cloned.1.call-done = bf16[96,2048]{1,0:T(8,128)(2,1)} async-done(((bf16[768,2048]{1,0:T(8,128)(2,1)}), bf16[96,2048]{1,0:T(8,128)(2,1)}) %reduce-scatter.5.cloned.1.call-update) | async-done | bytes 393232 | tf_op jit(solution)/shard_map/reduce_scatter | solution.py:192
  292.5 2.4 all_gather.7
  (118 shorter events, 49.5 us)
Async XLA Ops:
  6.5 62.1 %reduce-scatter.3.cloned.1.call-start = ((), (), s32[]{:S(2)}) async-start(), calls=%async_computation.2 | async-start | bytes 1179648 | tf_op jit(solution)/shard_map/reduce_scatter | solution.py:166
  8.6 15.2 %collective-permute-start.1 = (bf16[3,192,128]{2,1,0:T(8,128)(2,1)S(1)}, bf16[3,192,128]{2,1,0:T(8,128)(2,1)S(1)}, u32[]{:S(2)}, u32[]{:S(2)}) collective-permute-start(bf16[3,192,128]{2,1,0:T(8,128)(2,1)S(1)} %pad_maximum_fusion.11), channel_id=1, source_target_pairs={{0,16},{8,24},{16,0},{24,8},{1,17},{9,25},{17,1},{25,9},{2,18},{10... | collective-permute-start | bytes 442376 | tf_op jit(solution)/shard_map/ppermute | solution.py:86
  60.8 176.3 %all-gather.2.cloned.1.call-start = ((), (), s32[]{:S(2)}) async-start(), calls=%async_computation.3 | async-start | bytes 3538944 | tf_op jit(solution)/shard_map/all_gather | solution.py:175
  71.8 219.6 %reduce-scatter.5.cloned.1.call-start = ((), (), s32[]{:S(2)}) async-start(), calls=%async_computation.4 | async-start | bytes 3538944 | tf_op jit(solution)/shard_map/reduce_scatter | solution.py:192
  75.3 14.9 %collective-permute-start.26 = (bf16[768,128]{1,0:T(8,128)(2,1)S(1)}, bf16[768,128]{1,0:T(8,128)(2,1)S(1)}, u32[]{:S(2)}, u32[]{:S(2)}) collective-permute-start(bf16[768,128]{1,0:T(8,128)(2,1)S(1)} %get-tuple-element.9), channel_id=1, source_target_pairs={{0,24},{8,16},{16,8},{24,0},{1,25},{9,17},{17,9},{25,1},{2,26},{10... | collective-permute-start | bytes 589832 | tf_op jit(solution)/shard_map/ppermute | solution.py:86
  77.7 28.4 %collective-permute-start.25 = (bf16[768,128]{1,0:T(8,128)(2,1)S(1)}, bf16[768,128]{1,0:T(8,128)(2,1)S(1)}, u32[]{:S(2)}, u32[]{:S(2)}) collective-permute-start(bf16[768,128]{1,0:T(8,128)(2,1)S(1)} %get-tuple-element.10), channel_id=1, source_target_pairs={{0,16},{8,24},{16,0},{24,8},{1,17},{9,25},{17,1},{25,9},{2,18},{10... | collective-permute-start | bytes 589832 | tf_op jit(solution)/shard_map/ppermute | solution.py:86
  78.2 34.3 %collective-permute-start.18 = (bf16[128,768]{1,0:T(8,128)(2,1)S(1)}, bf16[128,768]{1,0:T(8,128)(2,1)S(1)}, u32[]{:S(2)}, u32[]{:S(2)}) collective-permute-start(bf16[128,768]{1,0:T(8,128)(2,1)S(1)} %get-tuple-element.12), channel_id=1, source_target_pairs={{0,8},{8,0},{16,24},{24,16},{1,9},{9,1},{17,25},{25,17},{2,10},{10... | collective-permute-start | bytes 589832 | tf_op jit(solution)/shard_map/ppermute | solution.py:86
  80.7 75.4 %collective-permute-start.12 = (bf16[128,768]{1,0:T(8,128)(2,1)S(1)}, bf16[128,768]{1,0:T(8,128)(2,1)S(1)}, u32[]{:S(2)}, u32[]{:S(2)}) collective-permute-start(bf16[128,768]{1,0:T(8,128)(2,1)S(1)} %get-tuple-element.16), channel_id=1, source_target_pairs={{0,8},{8,0},{16,24},{24,16},{1,9},{9,1},{17,25},{25,17},{2,10},{10... | collective-permute-start | bytes 589832 | tf_op jit(solution)/shard_map/ppermute | solution.py:86
  80.9 75.3 %collective-permute-start.14 = (bf16[128,768]{1,0:T(8,128)(2,1)S(1)}, bf16[128,768]{1,0:T(8,128)(2,1)S(1)}, u32[]{:S(2)}, u32[]{:S(2)}) collective-permute-start(bf16[128,768]{1,0:T(8,128)(2,1)S(1)} %get-tuple-element.17), channel_id=1, source_target_pairs={{0,24},{8,16},{16,8},{24,0},{1,25},{9,17},{17,9},{25,1},{2,26},{10... | collective-permute-start | bytes 589832 | tf_op jit(solution)/shard_map/ppermute | solution.py:86
  90.2 65.9 %collective-permute-start.13 = (bf16[128,768]{1,0:T(8,128)(2,1)S(1)}, bf16[128,768]{1,0:T(8,128)(2,1)S(1)}, u32[]{:S(2)}, u32[]{:S(2)}) collective-permute-start(bf16[128,768]{1,0:T(8,128)(2,1)S(1)} %get-tuple-element.18), channel_id=1, source_target_pairs={{0,16},{8,24},{16,0},{24,8},{1,17},{9,25},{17,1},{25,9},{2,18},{10... | collective-permute-start | bytes 589832 | tf_op jit(solution)/shard_map/ppermute | solution.py:86
  106.1 32.2 %collective-permute-start.20 = (bf16[128,768]{1,0:T(8,128)(2,1)S(1)}, bf16[128,768]{1,0:T(8,128)(2,1)S(1)}, u32[]{:S(2)}, u32[]{:S(2)}) collective-permute-start(bf16[128,768]{1,0:T(8,128)(2,1)S(1)} %get-tuple-element.13), channel_id=1, source_target_pairs={{0,24},{8,16},{16,8},{24,0},{1,25},{9,17},{17,9},{25,1},{2,26},{10... | collective-permute-start | bytes 589832 | tf_op jit(solution)/shard_map/ppermute | solution.py:86
  112.5 42.0 %collective-permute-start.19 = (bf16[128,768]{1,0:T(8,128)(2,1)S(1)}, bf16[128,768]{1,0:T(8,128)(2,1)S(1)}, u32[]{:S(2)}, u32[]{:S(2)}) collective-permute-start(bf16[128,768]{1,0:T(8,128)(2,1)S(1)} %get-tuple-element.14), channel_id=1, source_target_pairs={{0,16},{8,24},{16,0},{24,8},{1,17},{9,25},{17,1},{25,9},{2,18},{10... | collective-permute-start | bytes 589832 | tf_op jit(solution)/shard_map/ppermute | solution.py:86
  138.3 21.4 %collective-permute-start.29 = (bf16[4,384,128]{2,1,0:T(8,128)(2,1)S(1)}, bf16[4,384,128]{2,1,0:T(8,128)(2,1)S(1)}, u32[]{:S(2)}, u32[]{:S(2)}) collective-permute-start(bf16[4,384,128]{2,1,0:T(8,128)(2,1)S(1)} %get-tuple-element.5), channel_id=1, source_target_pairs={{0,4},{2,6},{4,0},{6,2},{1,5},{3,7},{5,1},{7,3},{8,12},{10,14},{12... | collective-permute-start | bytes 1179656 | tf_op jit(solution)/shard_map/ppermute | solution.py:86
  154.6 40.6 %collective-permute-start.22 = (bf16[512,768]{1,0:T(8,128)(2,1)S(1)}, bf16[512,768]{1,0:T(8,128)(2,1)}, u32[]{:S(2)}, u32[]{:S(2)}) collective-permute-start(bf16[512,768]{1,0:T(8,128)(2,1)S(1)} %bitcast.84), channel_id=1, source_target_pairs={{0,4},{2,6},{4,0},{6,2},{1,5},{3,7},{5,1},{7,3},{8,12},{10,14},{12... | collective-permute-start | bytes 2359304 | tf_op jit(solution)/shard_map/ppermute | solution.py:86
  157.1 39.5 %collective-permute-start.15 = (bf16[512,768]{1,0:T(8,128)(2,1)}, bf16[512,768]{1,0:T(8,128)(2,1)}, u32[]{:S(2)}, u32[]{:S(2)}) collective-permute-start(bf16[512,768]{1,0:T(8,128)(2,1)} %bitcast.45.refs_0_), channel_id=1, source_target_pairs={{0,2},{2,0},{4,6},{6,4},{1,3},{3,1},{5,7},{7,5},{8,10},{10,8},{12,... | collective-permute-start | bytes 2359304 | tf_op jit(solution)/shard_map/ppermute | solution.py:86
  158.6 27.6 %collective-permute-start.27 = (bf16[4,384,128]{2,1,0:T(8,128)(2,1)S(1)}, bf16[4,384,128]{2,1,0:T(8,128)(2,1)S(1)}, u32[]{:S(2)}, u32[]{:S(2)}) collective-permute-start(bf16[4,384,128]{2,1,0:T(8,128)(2,1)S(1)} %get-tuple-element.5), channel_id=1, source_target_pairs={{0,2},{2,0},{4,6},{6,4},{1,3},{3,1},{5,7},{7,5},{8,10},{10,8},{12,... | collective-permute-start | bytes 1179656 | tf_op jit(solution)/shard_map/ppermute | solution.py:86
  159.2 27.6 %collective-permute-start.30 = (bf16[4,384,128]{2,1,0:T(8,128)(2,1)S(1)}, bf16[4,384,128]{2,1,0:T(8,128)(2,1)}, u32[]{:S(2)}, u32[]{:S(2)}) collective-permute-start(bf16[4,384,128]{2,1,0:T(8,128)(2,1)S(1)} %get-tuple-element.6), channel_id=1, source_target_pairs={{0,4},{2,6},{4,0},{6,2},{1,5},{3,7},{5,1},{7,3},{8,12},{10,14},{12... | collective-permute-start | bytes 1179656 | tf_op jit(solution)/shard_map/ppermute | solution.py:86
  159.7 34.9 %collective-permute-start.28 = (bf16[4,384,128]{2,1,0:T(8,128)(2,1)S(1)}, bf16[4,384,128]{2,1,0:T(8,128)(2,1)S(1)}, u32[]{:S(2)}, u32[]{:S(2)}) collective-permute-start(bf16[4,384,128]{2,1,0:T(8,128)(2,1)S(1)} %get-tuple-element.6), channel_id=1, source_target_pairs={{0,2},{2,0},{4,6},{6,4},{1,3},{3,1},{5,7},{7,5},{8,10},{10,8},{12,... | collective-permute-start | bytes 1179656 | tf_op jit(solution)/shard_map/ppermute | solution.py:86
  186.2 11.9 %collective-permute-start.31 = (bf16[4,384,128]{2,1,0:T(8,128)(2,1)S(1)}, bf16[4,384,128]{2,1,0:T(8,128)(2,1)S(1)}, u32[]{:S(2)}, u32[]{:S(2)}) collective-permute-start(bf16[4,384,128]{2,1,0:T(8,128)(2,1)S(1)} %collective-permute-done.27), channel_id=1, source_target_pairs={{0,4},{2,6},{4,0},{6,2},{1,5},{3,7},{5,1},{7,3},{8,12},{10,14},{12... | collective-permute-start | bytes 1179656 | tf_op jit(solution)/shard_map/ppermute | solution.py:86
  186.7 50.3 %collective-permute-start.21 = (bf16[512,768]{1,0:T(8,128)(2,1)S(1)}, bf16[512,768]{1,0:T(8,128)(2,1)}, u32[]{:S(2)}, u32[]{:S(2)}) collective-permute-start(bf16[512,768]{1,0:T(8,128)(2,1)S(1)} %bitcast.85), channel_id=1, source_target_pairs={{0,2},{2,0},{4,6},{6,4},{1,3},{3,1},{5,7},{7,5},{8,10},{10,8},{12,... | collective-permute-start | bytes 2359304 | tf_op jit(solution)/shard_map/ppermute | solution.py:86
  194.6 42.4 %collective-permute-start.16 = (bf16[512,768]{1,0:T(8,128)(2,1)}, bf16[512,768]{1,0:T(8,128)(2,1)}, u32[]{:S(2)}, u32[]{:S(2)}) collective-permute-start(bf16[512,768]{1,0:T(8,128)(2,1)} %bitcast.45.refs_0_), channel_id=1, source_target_pairs={{0,4},{2,6},{4,0},{6,2},{1,5},{3,7},{5,1},{7,3},{8,12},{10,14},{12... | collective-permute-start | bytes 2359304 | tf_op jit(solution)/shard_map/ppermute | solution.py:86
  195.2 41.9 %collective-permute-start.23 = (bf16[512,768]{1,0:T(8,128)(2,1)}, bf16[512,768]{1,0:T(8,128)(2,1)}, u32[]{:S(2)}, u32[]{:S(2)}) collective-permute-start(bf16[512,768]{1,0:T(8,128)(2,1)} %collective-permute-done.22.refs_6_), channel_id=1, source_target_pairs={{0,2},{2,0},{4,6},{6,4},{1,3},{3,1},{5,7},{7,5},{8,10},{10,8},{12,... | collective-permute-start | bytes 2359304 | tf_op jit(solution)/shard_map/ppermute | solution.py:86
  196.7 40.4 %collective-permute-start.17 = (bf16[512,768]{1,0:T(8,128)(2,1)}, bf16[512,768]{1,0:T(8,128)(2,1)}, u32[]{:S(2)}, u32[]{:S(2)}) collective-permute-start(bf16[512,768]{1,0:T(8,128)(2,1)} %collective-permute-done.15.refs_1_), channel_id=1, source_target_pairs={{0,4},{2,6},{4,0},{6,2},{1,5},{3,7},{5,1},{7,3},{8,12},{10,14},{12... | collective-permute-start | bytes 2359304 | tf_op jit(solution)/shard_map/ppermute | solution.py:86
  198.9 36.2 %collective-permute-start.32 = (bf16[4,384,128]{2,1,0:T(8,128)(2,1)}, bf16[4,384,128]{2,1,0:T(8,128)(2,1)}, u32[]{:S(2)}, u32[]{:S(2)}) collective-permute-start(bf16[4,384,128]{2,1,0:T(8,128)(2,1)} %collective-permute-done.30), channel_id=1, source_target_pairs={{0,2},{2,0},{4,6},{6,4},{1,3},{3,1},{5,7},{7,5},{8,10},{10,8},{12,... | collective-permute-start | bytes 1179656 | tf_op jit(solution)/shard_map/ppermute | solution.py:86
  (28 other events, 373.4 us)
Sparse Core Ops, SparseCore 0:
  60.9 7.6 reduce-scatter.2
  71.9 75.7 all-gather.1
  251.8 39.4 reduce-scatter.4

commit v3 on v2

--- a/solution.py
+++ b/solution.py
@@ -50,35 +50,36 @@
         o_ref[z_self ^ zq] = (mixed * scale * gain_ref[...]).astype(BF)
 
 
-def mixer_kernel(pos_ref, x_ref, *refs, rows):
-    gates, ups, downs = refs[0:4], refs[4:8], refs[8:12]
-    o_ref = refs[12]
+def mixer_kernel(pos_ref, *refs, parts):
+    xs, refs = refs[:parts], refs[parts:]
+    gates, ups, downs, outs = refs[0:4], refs[4:8], refs[8:12], refs[12:]
     z_self, p_self, first_unit = pos_ref[0], pos_ref[1], pos_ref[2]
     block = downs[0].shape[2]
     span = gates[0].shape[1]
+    own = xs[0].shape[0]
+    rows = own * parts
 
     def lanes(i, j):
         return pl.ds(pl.multiple_of(((z_self ^ j) * 4 + (p_self ^ i)) * block, block), block)
 
-    def step(n, carry):
-        at = pl.ds(pl.multiple_of(n * rows, rows), rows)
-        gate = jnp.zeros((rows, span), F32)
-        up = jnp.zeros((rows, span), F32)
-        for i in range(4):
-            x = jnp.concatenate([x_ref[at, lanes(i, j)] for j in range(4)], axis=1)
-            gate = gate + jnp.dot(x, gates[i][...], preferred_element_type=F32)
-            up = up + jnp.dot(x, ups[i][...], preferred_element_type=F32)
-        hidden = gate / (1.0 + jnp.exp(-gate)) * up
-        keep = lax.broadcasted_iota(jnp.int32, (rows, span), 1) >= first_unit
-        hidden = jnp.where(keep, hidden, 0.0).astype(BF)
-        for i in range(4):
-            down = jnp.concatenate([downs[i][j] for j in range(4)], axis=1)
-            out = jnp.dot(hidden, down, preferred_element_type=F32).astype(BF)
-            for j in range(4):
-                o_ref[at, lanes(i, j)] = out[:, j * block : (j + 1) * block]
-        return carry
-
-    lax.fori_loop(0, x_ref.shape[0] // rows, step, 0)
+    gate = jnp.zeros((rows, span), F32)
+    up = jnp.zeros((rows, span), F32)
+    for i in range(4):
+        x = jnp.concatenate(
+            [jnp.concatenate([x_ref[:, lanes(i, j)] for x_ref in xs], axis=0) for j in range(4)],
+            axis=1,
+        )
+        gate = gate + jnp.dot(x, gates[i][...], preferred_element_type=F32)
+        up = up + jnp.dot(x, ups[i][...], preferred_element_type=F32)
+    hidden = gate / (1.0 + jnp.exp(-gate)) * up
+    keep = lax.broadcasted_iota(jnp.int32, (rows, span), 1) >= first_unit
+    hidden = jnp.where(keep, hidden, 0.0).astype(BF)
+    for i in range(4):
+        down = jnp.concatenate([downs[i][j] for j in range(4)], axis=1)
+        out = jnp.dot(hidden, down, preferred_element_type=F32).astype(BF)
+        for j in range(4):
+            for n, o_ref in enumerate(outs):
+                o_ref[:, lanes(i, j)] = out[n * own : (n + 1) * own, j * block : (j + 1) * block]
 
 
 def swap(x, axis, bit):
@@ -144,7 +145,7 @@
     smem = pl.BlockSpec(memory_space=pltpu.SMEM)
     vmem = pl.BlockSpec(memory_space=pltpu.VMEM)
     keys_total = 16 * tok_rows
-    out = pl.pallas_call(
+    attend = pl.pallas_call(
         functools.partial(attn_kernel, groups=4, planes=4, rows=tok_rows),
         out_shape=jax.ShapeDtypeStruct((4, tok_rows, VD), BF),
         in_specs=[smem, smem, vmem, vmem, vmem, vmem],
@@ -157,39 +158,63 @@
         ),
         compiler_params=pltpu.CompilerParams(vmem_limit_bytes=40 * 1024 * 1024),
         name="attn",
-    )(jnp.stack([z_self, p_self]), lam, qkv[:, 2], key_all, value_all, head_gain.reshape(1, VD))
+    )
+    place = jnp.stack([z_self, p_self])
+    out = attend(place, lam, qkv[:, 2], key_all, value_all, head_gain.reshape(1, VD))
     back = z_exchange(lambda g: lax.dynamic_index_in_dim(out, g ^ z_self, 0, keepdims=False))
     head_out = jnp.concatenate(
         [lax.dynamic_index_in_dim(back, z_self ^ h, 0, keepdims=False) for h in range(4)], axis=1
     )
     projected = jnp.dot(head_out, out_weight, preferred_element_type=F32).astype(BF)
-    branch = lax.psum_scatter(
-        projected,
-        "tp",
-        scatter_dimension=0,
-        tiled=True,
-    ).astype(F32)
-    resid_own = lax.dynamic_slice_in_dim(resid, lax.axis_index("tp") * own_rows, own_rows, 0)
-    first = resid_own.astype(F32) + branch
-    normed = first * lax.rsqrt(jnp.mean(first * first, axis=-1, keepdims=True) + 1e-06) * norm_gain
-    normed_all = lax.all_gather(normed.astype(BF), ("z", "tp"), axis=0, tiled=True)
+    t_self = lax.axis_index("tp")
+
+    def half_rows(x, t):
+        return lax.dynamic_slice_in_dim(x, t * own_rows, own_rows, 0)
+
+    branch_in = swap(half_rows(projected, 1 - t_self), "tp", 1)
+    branch = half_rows(projected, t_self).astype(F32) + branch_in.astype(F32)
+    first = half_rows(resid, t_self).astype(F32) + branch
+    scale = lax.rsqrt(jnp.mean(first * first, axis=-1, keepdims=True) + 1e-06)
+    normed = (first * scale * norm_gain).astype(BF)
+    mine = [normed] + [None] * 3
+    for j in (3, 2, 1):
+        mine[j] = swap(normed, "z", j)
+    other = [swap(x, "tp", 1) for x in mine]
     first_unit = z_self * span - start(z_self)
-    tokens = normed_all.shape[0]
-    step = 256 if tokens % 256 == 0 else tokens
-    terms = pl.pallas_call(
-        functools.partial(mixer_kernel, rows=step),
-        out_shape=jax.ShapeDtypeStruct((tokens, width), BF),
-        in_specs=[smem] + [vmem] * 13,
-        out_specs=vmem,
-        cost_estimate=pl.CostEstimate(
-            flops=6 * tokens * width * span,
-            transcendentals=tokens * span,
-            bytes_accessed=6 * width * span + 4 * tokens * width,
-        ),
-        compiler_params=pltpu.CompilerParams(vmem_limit_bytes=50 * 1024 * 1024),
-        name="mixer",
-    )(jnp.stack([z_self, p_self, first_unit]), normed_all, *gates, *ups, *downs)
-    mixer = lax.psum_scatter(terms, ("z", "tp"), scatter_dimension=0, tiled=True).astype(F32)
+    pos = jnp.stack([z_self, p_self, first_unit])
+
+    def mix(slots):
+        tokens = len(slots) * 2 * own_rows
+        xs = [x for j in slots for x in (mine[j], other[j])]
+        return pl.pallas_call(
+            functools.partial(mixer_kernel, parts=len(xs)),
+            out_shape=[jax.ShapeDtypeStruct((own_rows, width), BF)] * len(xs),
+            in_specs=[smem] + [vmem] * (12 + len(xs)),
+            out_specs=[vmem] * len(xs),
+            cost_estimate=pl.CostEstimate(
+                flops=6 * tokens * width * span,
+                transcendentals=tokens * span,
+                bytes_accessed=6 * width * span + 4 * tokens * width,
+            ),
+            compiler_params=pltpu.CompilerParams(vmem_limit_bytes=50 * 1024 * 1024),
+            name="mixer",
+        )(pos, *xs, *gates, *ups, *downs)
+
+    def summed(keep, give):
+        got = swap(give, "tp", 1)
+        return keep.astype(F32) + got.astype(F32)
+
+    far = mix((3, 2))
+    sums = []
+    for n, j in enumerate((3, 2)):
+        part = summed(far[2 * n], far[2 * n + 1]).astype(BF)
+        sums.append(swap(part, "z", j))
+    near = mix((1, 0))
+    part = summed(near[0], near[1]).astype(BF)
+    sums.append(swap(part, "z", 1))
+    mixer = summed(near[2], near[3])
+    for part in sums:
+        mixer = mixer + part.astype(F32)
     finished = (first + 0.5 * mixer).astype(BF)
     return lax.all_gather(finished, "tp", axis=0, tiled=True)
 

time: 303 us -> 229 us (0.76)
  waiting for transfers between devices: 181 us -> 102 us
  between operations: 13.4 us -> 0.46 us
  local copies, waits for them, and re-layouts: 7.08 us -> 17.3 us
  starting transfers between devices: 63.7 us -> 71.6 us
    reduce_scatter x2 -> x0, waiting for transfers between devices: 47.4 us -> none  [the longest x1 39.7 us: fast_local(): lax.psum_scatter(terms, ('z', 'tp'), scatter_dimension=0, tiled=True)]
    ppermute x33 -> x48, waiting for transfers between devices: 133 us -> 102 us  [swap(): return lax.ppermute(x, axis, [(i, i ^ bit) for i in range(size)])]
    ppermute x33 -> x48, starting transfers between devices: 63.5 us -> 71.6 us  [swap(): return lax.ppermute(x, axis, [(i, i ^ bit) for i in range(size)])]
    another operation x6, other arithmetic: 1.3 us -> 6.74 us  [z_exchange(): return jnp.stack([part(z_self)] + got)]
    concatenate x3 -> x0, other arithmetic: 4.98 us -> none  [fast_local(): downs = [jnp.concatenate(pair, axis=1) for pair in zip(low, high)]]
    unnamed x33 -> x68, local copies, waits for them, and re-layouts: 1.72 us -> 5.85 us
    pallas_call x2 -> x3, Pallas kernels: 21.4 us -> 21.8 us  [the longest x2 15.1 us: mix(): pl.pallas_call(functools.partial(mixer_kernel, parts=len(xs)), out_shape=...]
  transfers between devices with their start and end apart: 36 -> 48, of which waited for: 16 -> 13; matrix products, arithmetic and copies ran while one was open for 3% -> 10% of each run, Pallas kernels for 0% -> 10%
where the time goes in v3:
time: 229 us; the launch traced here: 228 us
  waiting for transfers between devices  102 us (45%)
  starting transfers between devices  71.6 us (31%)
  Pallas kernels  21.8 us (10%)
  local copies, waits for them, and re-layouts  17.3 us (8%)
  other arithmetic  12.4 us (5%)
  blocking collectives  2.37 us (1%)
    ppermute x48, waiting for transfers between devices, swap(): return lax.ppermute(x, axis, [(i, i ^ bit) for i in range(size)])  102 us
    ppermute x48, starting transfers between devices, swap(): return lax.ppermute(x, axis, [(i, i ^ bit) for i in range(size)])  71.6 us
    pallas_call x2, Pallas kernels, mix(): pl.pallas_call(functools.partial(mixer_kernel, parts=len(xs)), out_shape=...  15.1 us
    pallas_call x1, Pallas kernels, fast_local(): attend(place, lam, qkv[:, 2], key_all, value_all, head_gain.reshape(1, VD))  6.75 us
    another operation x6, other arithmetic, z_exchange(): return jnp.stack([part(z_self)] + got)  6.74 us
    unnamed x68, local copies, waits for them, and re-layouts  5.85 us
  transfers between devices with their start and end apart: 48, of which 13 were waited for; matrix products, arithmetic and copies ran while one was open for 10% of the time, Pallas kernels for 10%

profile of v3, /device:TPU:0, one launch (start us, length us, event | category | flops | bytes accessed | tf_op | source)
XLA Modules:
  0.0 228.2 jit_solution(8380709825992544976)
XLA Ops:
  4.0 3.1 %collective-permute-start = (bf16[3,192,128]{2,1,0:T(8,128)(2,1)}, bf16[3,192,128]{2,1,0:T(8,128)(2,1)}, u32[]{:S(2)}, u32[]{:S(2)}) collective-permute-start(bf16[3,192,128]{2,1,0:T(8,128)(2,1)} %pad_maximum_fusion.7), channel_id=1, source_target_pairs={{0,8},{8,0},{16,24},{24,16},{1,9},{9,1},{17,25},{25,17},{2,10},{10... | collective-permute-start | bytes 442376 | tf_op jit(solution)/shard_map/ppermute | solution.py:87
  7.8 2.6 %collective-permute-start.1 = (bf16[3,192,128]{2,1,0:T(8,128)(2,1)}, bf16[3,192,128]{2,1,0:T(8,128)(2,1)}, u32[]{:S(2)}, u32[]{:S(2)}) collective-permute-start(bf16[3,192,128]{2,1,0:T(8,128)(2,1)} %pad_maximum_fusion.8), channel_id=1, source_target_pairs={{0,16},{8,24},{16,0},{24,8},{1,17},{9,25},{17,1},{25,9},{2,18},{10... | collective-permute-start | bytes 442376 | tf_op jit(solution)/shard_map/ppermute | solution.py:87
  12.9 3.5 %collective-permute-start.29 = (bf16[768,128]{1,0:T(8,128)(2,1)}, bf16[768,128]{1,0:T(8,128)(2,1)}, u32[]{:S(2)}, u32[]{:S(2)}) collective-permute-start(bf16[768,128]{1,0:T(8,128)(2,1)} %get-tuple-element.26), channel_id=1, source_target_pairs={{0,16},{8,24},{16,0},{24,8},{1,17},{9,25},{17,1},{25,9},{2,18},{10... | collective-permute-start | bytes 589832 | tf_op jit(solution)/shard_map/ppermute | solution.py:87
  18.0 4.0 %collective-permute-done.1 = bf16[3,192,128]{2,1,0:T(8,128)(2,1)} collective-permute-done((bf16[3,192,128]{2,1,0:T(8,128)(2,1)}, bf16[3,192,128]{2,1,0:T(8,128)(2,1)}, u32[]{:S(2)}, u32[]{:S(2)}) %collective-permute-start.1) | collective-permute-done | bytes 147488 | tf_op jit(solution)/shard_map/ppermute | solution.py:87
  30.7 7.0 %collective-permute-done.29 = bf16[768,128]{1,0:T(8,128)(2,1)} collective-permute-done((bf16[768,128]{1,0:T(8,128)(2,1)}, bf16[768,128]{1,0:T(8,128)(2,1)}, u32[]{:S(2)}, u32[]{:S(2)}) %collective-permute-start.29) | collective-permute-done | bytes 196640 | tf_op jit(solution)/shard_map/ppermute | solution.py:87
  37.7 5.1 %collective-permute-start.16 = (bf16[128,768]{1,0:T(8,128)(2,1)S(1)}, bf16[128,768]{1,0:T(8,128)(2,1)S(1)}, u32[]{:S(2)}, u32[]{:S(2)}) collective-permute-start(bf16[128,768]{1,0:T(8,128)(2,1)S(1)} %get-tuple-element.32), channel_id=1, source_target_pairs={{0,8},{8,0},{16,24},{24,16},{1,9},{9,1},{17,25},{25,17},{2,10},{10... | collective-permute-start | bytes 589832 | tf_op jit(solution)/shard_map/ppermute | solution.py:87
  50.7 6.7 %attn.1 = bf16[4,192,128]{2,1,0:T(8,128)(2,1)S(1)} custom-call(s32[2]{0:T(128)S(1)} %pad_add_fusion.pos_ref, f32[1]{0:T(128)} %dynamic_slice.110.lam_ref, bf16[4,192,128]{2,1,0:T(8,128)(2,1)S(1)} %get-tuple-element.39.q_ref, bf16[4,4,192,128]{3,2,1,0:T(8,128)(2,1)S(1)} %pad_maximum_fusion.k_ref, bf16[4,4,192,128]{3,2,1,0:T(8,128)(2,1)S(1)} %pad_maximum_fusion.1.v_ref, ...), custom_call_target="tpu_custom_call" | custom-call | flops 1811939328 | bytes 1572864 | tf_op jit(solution)/shard_map/attn/pallas_call | solution.py:163
  58.0 2.6 %collective-permute-start.10 = (bf16[192,128]{1,0:T(8,128)(2,1)S(1)}, bf16[192,128]{1,0:T(8,128)(2,1)S(1)}, u32[]{:S(2)}, u32[]{:S(2)}) collective-permute-start(bf16[192,128]{1,0:T(8,128)(2,1)S(1)} %get-tuple-element.46), channel_id=1, source_target_pairs={{0,16},{8,24},{16,0},{24,8},{1,17},{9,25},{17,1},{25,9},{2,18},{10... | collective-permute-start | bytes 147464 | tf_op jit(solution)/shard_map/ppermute | solution.py:87
  62.9 3.8 %collective-permute-start.18 = (bf16[128,768]{1,0:T(8,128)(2,1)S(1)}, bf16[128,768]{1,0:T(8,128)(2,1)S(1)}, u32[]{:S(2)}, u32[]{:S(2)}) collective-permute-start(bf16[128,768]{1,0:T(8,128)(2,1)S(1)} %get-tuple-element.33), channel_id=1, source_target_pairs={{0,24},{8,16},{16,8},{24,0},{1,25},{9,17},{17,9},{25,1},{2,26},{10... | collective-permute-start | bytes 589832 | tf_op jit(solution)/shard_map/ppermute | solution.py:87
  69.7 2.5 %collective-permute-start.31 = (bf16[4,384,128]{2,1,0:T(8,128)(2,1)}, bf16[4,384,128]{2,1,0:T(8,128)(2,1)}, u32[]{:S(2)}, u32[]{:S(2)}) collective-permute-start(bf16[4,384,128]{2,1,0:T(8,128)(2,1)} %get-tuple-element.22), channel_id=1, source_target_pairs={{0,2},{2,0},{4,6},{6,4},{1,3},{3,1},{5,7},{7,5},{8,10},{10,8},{12,... | collective-permute-start | bytes 1179656 | tf_op jit(solution)/shard_map/ppermute | solution.py:87
  74.7 4.4 %collective-permute-done.23 = bf16[128,768]{1,0:T(8,128)(2,1)S(1)} collective-permute-done((bf16[128,768]{1,0:T(8,128)(2,1)S(1)}, bf16[128,768]{1,0:T(8,128)(2,1)S(1)}, u32[]{:S(2)}, u32[]{:S(2)}) %collective-permute-start.23) | collective-permute-done | bytes 196640 | tf_op jit(solution)/shard_map/ppermute | solution.py:87
  83.0 4.1 %collective-permute-done.24 = bf16[128,768]{1,0:T(8,128)(2,1)} collective-permute-done((bf16[128,768]{1,0:T(8,128)(2,1)}, bf16[128,768]{1,0:T(8,128)(2,1)}, u32[]{:S(2)}, u32[]{:S(2)}) %collective-permute-start.24) | collective-permute-done | bytes 196640 | tf_op jit(solution)/shard_map/ppermute | solution.py:87
  91.2 2.5 %collective-permute-start.19 = (bf16[512,768]{1,0:T(8,128)(2,1)S(1)}, bf16[512,768]{1,0:T(8,128)(2,1)S(1)}, u32[]{:S(2)}, u32[]{:S(2)}) collective-permute-start(bf16[512,768]{1,0:T(8,128)(2,1)S(1)} %bitcast.84), channel_id=1, source_target_pairs={{0,2},{2,0},{4,6},{6,4},{1,3},{3,1},{5,7},{7,5},{8,10},{10,8},{12,... | collective-permute-start | bytes 2359304 | tf_op jit(solution)/shard_map/ppermute | solution.py:87
  99.3 2.5 %collective-permute-start.25 = (bf16[512,768]{1,0:T(8,128)(2,1)}, bf16[512,768]{1,0:T(8,128)(2,1)}, u32[]{:S(2)}, u32[]{:S(2)}) collective-permute-start(bf16[512,768]{1,0:T(8,128)(2,1)} %bitcast.50.refs_8_), channel_id=1, source_target_pairs={{0,2},{2,0},{4,6},{6,4},{1,3},{3,1},{5,7},{7,5},{8,10},{10,8},{12,... | collective-permute-start | bytes 2359304 | tf_op jit(solution)/shard_map/ppermute | solution.py:87
  101.7 5.9 %collective-permute-done.35 = bf16[4,384,128]{2,1,0:T(8,128)(2,1)S(1)} collective-permute-done((bf16[4,384,128]{2,1,0:T(8,128)(2,1)}, bf16[4,384,128]{2,1,0:T(8,128)(2,1)S(1)}, u32[]{:S(2)}, u32[]{:S(2)}) %collective-permute-start.35) | collective-permute-done | bytes 393248 | tf_op jit(solution)/shard_map/ppermute | solution.py:87
  107.7 2.5 %collective-permute-start.36 = (bf16[4,384,128]{2,1,0:T(8,128)(2,1)}, bf16[4,384,128]{2,1,0:T(8,128)(2,1)S(1)}, u32[]{:S(2)}, u32[]{:S(2)}) collective-permute-start(bf16[4,384,128]{2,1,0:T(8,128)(2,1)} %collective-permute-done.34), channel_id=1, source_target_pairs={{0,2},{2,0},{4,6},{6,4},{1,3},{3,1},{5,7},{7,5},{8,10},{10,8},{12,... | collective-permute-start | bytes 1179656 | tf_op jit(solution)/shard_map/ppermute | solution.py:87
  111.4 21.0 %collective-permute-done.36 = bf16[4,384,128]{2,1,0:T(8,128)(2,1)S(1)} collective-permute-done((bf16[4,384,128]{2,1,0:T(8,128)(2,1)}, bf16[4,384,128]{2,1,0:T(8,128)(2,1)S(1)}, u32[]{:S(2)}, u32[]{:S(2)}) %collective-permute-start.36) | collective-permute-done | bytes 393248 | tf_op jit(solution)/shard_map/ppermute | solution.py:87
  135.5 5.1 %collective-permute-start.40 = (bf16[96,2048]{1,0:T(8,128)(2,1)S(1)}, bf16[96,2048]{1,0:T(8,128)(2,1)}, u32[]{:S(2)}, u32[]{:S(2)}) collective-permute-start(bf16[96,2048]{1,0:T(8,128)(2,1)S(1)} %multiply_convert_fusion.refs_2_), channel_id=1, source_target_pairs={{0,16},{8,24},{16,0},{24,8},{1,17},{9,25},{17,1},{25,9},{2,18},{10... | collective-permute-start | bytes 1179656 | tf_op jit(solution)/shard_map/ppermute | solution.py:87
  146.0 2.5 %collective-permute-start.13 = (bf16[96,2048]{1,0:T(8,128)(2,1)S(1)}, bf16[96,2048]{1,0:T(8,128)(2,1)S(1)}, u32[]{:S(2)}, u32[]{:S(2)}) collective-permute-start(bf16[96,2048]{1,0:T(8,128)(2,1)S(1)} %multiply_convert_fusion.refs_2_), channel_id=1, source_target_pairs={{0,8},{8,0},{16,24},{24,16},{1,9},{9,1},{17,25},{25,17},{2,10},{10... | collective-permute-start | bytes 1179656 | tf_op jit(solution)/shard_map/ppermute | solution.py:87
  148.6 18.7 %collective-permute-done.40.refs_2_ = bf16[96,2048]{1,0:T(8,128)(2,1)} collective-permute-done((bf16[96,2048]{1,0:T(8,128)(2,1)S(1)}, bf16[96,2048]{1,0:T(8,128)(2,1)}, u32[]{:S(2)}, u32[]{:S(2)}) %collective-permute-start.40) | collective-permute-done | bytes 393248 | tf_op jit(solution)/shard_map/ppermute | solution.py:87
  172.4 7.7 %mixer.3 = (bf16[96,2048]{1,0:T(8,128)(2,1)S(1)}, bf16[96,2048]{1,0:T(8,128)(2,1)S(1)}, bf16[96,2048]{1,0:T(8,128)(2,1)S(1)}, bf16[96,2048]{1,0:T(8,128)(2,1)S(1)}) custom-call(s32[3]{0:T(128)S(1)} %pad_add_fusion.1.pos_ref, bf16[96,2048]{1,0:T(8,128)(2,1)} %collective-permute-done.38.refs_0_, bf16[96,2048]{1,0:T(8,128)(2,1)S(1)} %collective-permute-done.39.refs_1_, ...), custom_call_target="tpu_custom_call" | custom-call | flops 3623878656 | bytes 12582912 | tf_op jit(solution)/shard_map/mixer/pallas_call | solution.py:189
  180.7 7.4 %mixer.2 = (bf16[96,2048]{1,0:T(8,128)(2,1)S(1)}, bf16[96,2048]{1,0:T(8,128)(2,1)S(1)}, bf16[96,2048]{1,0:T(8,128)(2,1)S(1)}, bf16[96,2048]{1,0:T(8,128)(2,1)S(1)}) custom-call(s32[3]{0:T(128)S(1)} %pad_add_fusion.1.pos_ref, bf16[96,2048]{1,0:T(8,128)(2,1)S(1)} %collective-permute-done.13.refs_0_, bf16[96,2048]{1,0:T(8,128)(2,1)S(1)} %collective-permute-done.14.refs_1_, ...), custom_call_target="tpu_custom_call" | custom-call | flops 3623878656 | bytes 12582912 | tf_op jit(solution)/shard_map/mixer/pallas_call | solution.py:189
  193.6 9.2 %collective-permute-done.43 = bf16[96,2048]{1,0:T(8,128)(2,1)S(1)} collective-permute-done((bf16[96,2048]{1,0:T(8,128)(2,1)S(1)}, bf16[96,2048]{1,0:T(8,128)(2,1)S(1)}, u32[]{:S(2)}, u32[]{:S(2)}) %collective-permute-start.43) | collective-permute-done | bytes 393248 | tf_op jit(solution)/shard_map/ppermute | solution.py:87
  202.8 21.6 %collective-permute-done.45 = bf16[96,2048]{1,0:T(8,128)(2,1)S(1)} collective-permute-done((bf16[96,2048]{1,0:T(8,128)(2,1)S(1)}, bf16[96,2048]{1,0:T(8,128)(2,1)S(1)}, u32[]{:S(2)}, u32[]{:S(2)}) %collective-permute-start.45) | collective-permute-done | bytes 393248 | tf_op jit(solution)/shard_map/ppermute | solution.py:87
  (179 shorter events, 71.7 us)
Async XLA Ops:
  12.9 24.8 %collective-permute-start.29 = (bf16[768,128]{1,0:T(8,128)(2,1)}, bf16[768,128]{1,0:T(8,128)(2,1)}, u32[]{:S(2)}, u32[]{:S(2)}) collective-permute-start(bf16[768,128]{1,0:T(8,128)(2,1)} %get-tuple-element.26), channel_id=1, source_target_pairs={{0,16},{8,24},{16,0},{24,8},{1,17},{9,25},{17,1},{25,9},{2,18},{10... | collective-permute-start | bytes 589832 | tf_op jit(solution)/shard_map/ppermute | solution.py:87
  17.9 25.0 %collective-permute-start.30 = (bf16[768,128]{1,0:T(8,128)(2,1)}, bf16[768,128]{1,0:T(8,128)(2,1)S(1)}, u32[]{:S(2)}, u32[]{:S(2)}) collective-permute-start(bf16[768,128]{1,0:T(8,128)(2,1)} %get-tuple-element.25), channel_id=1, source_target_pairs={{0,24},{8,16},{16,8},{24,0},{1,25},{9,17},{17,9},{25,1},{2,26},{10... | collective-permute-start | bytes 589832 | tf_op jit(solution)/shard_map/ppermute | solution.py:87
  26.0 18.3 %collective-permute-start.3 = (bf16[4,192,128]{2,1,0:T(8,128)(2,1)S(1)}, bf16[4,192,128]{2,1,0:T(8,128)(2,1)S(1)}, u32[]{:S(2)}, u32[]{:S(2)}) collective-permute-start(bf16[4,192,128]{2,1,0:T(8,128)(2,1)S(1)} %get-tuple-element.36), channel_id=1, source_target_pairs={{0,2},{2,0},{4,6},{6,4},{1,3},{3,1},{5,7},{7,5},{8,10},{10,8},{12,... | collective-permute-start | bytes 589832 | tf_op jit(solution)/shard_map/ppermute | solution.py:87
  28.6 17.4 %collective-permute-start.6 = (bf16[4,192,128]{2,1,0:T(8,128)(2,1)S(1)}, bf16[4,192,128]{2,1,0:T(8,128)(2,1)S(1)}, u32[]{:S(2)}, u32[]{:S(2)}) collective-permute-start(bf16[4,192,128]{2,1,0:T(8,128)(2,1)S(1)} %get-tuple-element.37), channel_id=1, source_target_pairs={{0,2},{2,0},{4,6},{6,4},{1,3},{3,1},{5,7},{7,5},{8,10},{10,8},{12,... | collective-permute-start | bytes 589832 | tf_op jit(solution)/shard_map/ppermute | solution.py:87
  29.1 18.2 %collective-permute-start.8 = (bf16[4,192,128]{2,1,0:T(8,128)(2,1)S(1)}, bf16[4,192,128]{2,1,0:T(8,128)(2,1)S(1)}, u32[]{:S(2)}, u32[]{:S(2)}) collective-permute-start(bf16[4,192,128]{2,1,0:T(8,128)(2,1)S(1)} %collective-permute-done.7), channel_id=1, source_target_pairs={{0,2},{2,0},{4,6},{6,4},{1,3},{3,1},{5,7},{7,5},{8,10},{10,8},{12,... | collective-permute-start | bytes 589832 | tf_op jit(solution)/shard_map/ppermute | solution.py:87
  37.7 32.0 %collective-permute-start.16 = (bf16[128,768]{1,0:T(8,128)(2,1)S(1)}, bf16[128,768]{1,0:T(8,128)(2,1)S(1)}, u32[]{:S(2)}, u32[]{:S(2)}) collective-permute-start(bf16[128,768]{1,0:T(8,128)(2,1)S(1)} %get-tuple-element.32), channel_id=1, source_target_pairs={{0,8},{8,0},{16,24},{24,16},{1,9},{9,1},{17,25},{25,17},{2,10},{10... | collective-permute-start | bytes 589832 | tf_op jit(solution)/shard_map/ppermute | solution.py:87
  46.0 26.2 %collective-permute-start.17 = (bf16[128,768]{1,0:T(8,128)(2,1)S(1)}, bf16[128,768]{1,0:T(8,128)(2,1)S(1)}, u32[]{:S(2)}, u32[]{:S(2)}) collective-permute-start(bf16[128,768]{1,0:T(8,128)(2,1)S(1)} %get-tuple-element.34), channel_id=1, source_target_pairs={{0,16},{8,24},{16,0},{24,8},{1,17},{9,25},{17,1},{25,9},{2,18},{10... | collective-permute-start | bytes 589832 | tf_op jit(solution)/shard_map/ppermute | solution.py:87
  69.7 19.0 %collective-permute-start.31 = (bf16[4,384,128]{2,1,0:T(8,128)(2,1)}, bf16[4,384,128]{2,1,0:T(8,128)(2,1)}, u32[]{:S(2)}, u32[]{:S(2)}) collective-permute-start(bf16[4,384,128]{2,1,0:T(8,128)(2,1)} %get-tuple-element.22), channel_id=1, source_target_pairs={{0,2},{2,0},{4,6},{6,4},{1,3},{3,1},{5,7},{7,5},{8,10},{10,8},{12,... | collective-permute-start | bytes 1179656 | tf_op jit(solution)/shard_map/ppermute | solution.py:87
  72.2 18.9 %collective-permute-start.34 = (bf16[4,384,128]{2,1,0:T(8,128)(2,1)}, bf16[4,384,128]{2,1,0:T(8,128)(2,1)}, u32[]{:S(2)}, u32[]{:S(2)}) collective-permute-start(bf16[4,384,128]{2,1,0:T(8,128)(2,1)} %get-tuple-element.21), channel_id=1, source_target_pairs={{0,4},{2,6},{4,0},{6,2},{1,5},{3,7},{5,1},{7,3},{8,12},{10,14},{12... | collective-permute-start | bytes 1179656 | tf_op jit(solution)/shard_map/ppermute | solution.py:87
  74.6 19.1 %collective-permute-start.32 = (bf16[4,384,128]{2,1,0:T(8,128)(2,1)}, bf16[4,384,128]{2,1,0:T(8,128)(2,1)}, u32[]{:S(2)}, u32[]{:S(2)}) collective-permute-start(bf16[4,384,128]{2,1,0:T(8,128)(2,1)} %get-tuple-element.21), channel_id=1, source_target_pairs={{0,2},{2,0},{4,6},{6,4},{1,3},{3,1},{5,7},{7,5},{8,10},{10,8},{12,... | collective-permute-start | bytes 1179656 | tf_op jit(solution)/shard_map/ppermute | solution.py:87
  74.7 20.6 %collective-permute-start.12 = (bf16[96,2048]{1,0:T(8,128)(2,1)}, bf16[96,2048]{1,0:T(8,128)(2,1)S(1)}, u32[]{:S(2)}, u32[]{:S(2)}) collective-permute-start(bf16[96,2048]{1,0:T(8,128)(2,1)} %constant_dynamic-slice_fusion.9), channel_id=1, source_target_pairs={{0,1},{1,0},{2,3},{3,2},{4,5},{5,4},{6,7},{7,6},{8,9},{9,8},{10,11... | collective-permute-start | bytes 1179656 | tf_op jit(solution)/shard_map/ppermute | solution.py:87
  88.7 19.0 %collective-permute-start.35 = (bf16[4,384,128]{2,1,0:T(8,128)(2,1)}, bf16[4,384,128]{2,1,0:T(8,128)(2,1)S(1)}, u32[]{:S(2)}, u32[]{:S(2)}) collective-permute-start(bf16[4,384,128]{2,1,0:T(8,128)(2,1)} %collective-permute-done.31), channel_id=1, source_target_pairs={{0,4},{2,6},{4,0},{6,2},{1,5},{3,7},{5,1},{7,3},{8,12},{10,14},{12... | collective-permute-start | bytes 1179656 | tf_op jit(solution)/shard_map/ppermute | solution.py:87
  91.2 43.4 %collective-permute-start.19 = (bf16[512,768]{1,0:T(8,128)(2,1)S(1)}, bf16[512,768]{1,0:T(8,128)(2,1)S(1)}, u32[]{:S(2)}, u32[]{:S(2)}) collective-permute-start(bf16[512,768]{1,0:T(8,128)(2,1)S(1)} %bitcast.84), channel_id=1, source_target_pairs={{0,2},{2,0},{4,6},{6,4},{1,3},{3,1},{5,7},{7,5},{8,10},{10,8},{12,... | collective-permute-start | bytes 2359304 | tf_op jit(solution)/shard_map/ppermute | solution.py:87
  93.7 48.5 %collective-permute-start.20 = (bf16[512,768]{1,0:T(8,128)(2,1)S(1)}, bf16[512,768]{1,0:T(8,128)(2,1)}, u32[]{:S(2)}, u32[]{:S(2)}) collective-permute-start(bf16[512,768]{1,0:T(8,128)(2,1)S(1)} %bitcast.85), channel_id=1, source_target_pairs={{0,4},{2,6},{4,0},{6,2},{1,5},{3,7},{5,1},{7,3},{8,12},{10,14},{12... | collective-permute-start | bytes 2359304 | tf_op jit(solution)/shard_map/ppermute | solution.py:87
  95.3 45.4 %collective-permute-start.26 = (bf16[512,768]{1,0:T(8,128)(2,1)}, bf16[512,768]{1,0:T(8,128)(2,1)}, u32[]{:S(2)}, u32[]{:S(2)}) collective-permute-start(bf16[512,768]{1,0:T(8,128)(2,1)} %bitcast.50.refs_8_), channel_id=1, source_target_pairs={{0,4},{2,6},{4,0},{6,2},{1,5},{3,7},{5,1},{7,3},{8,12},{10,14},{12... | collective-permute-start | bytes 2359304 | tf_op jit(solution)/shard_map/ppermute | solution.py:87
  99.3 46.8 %collective-permute-start.25 = (bf16[512,768]{1,0:T(8,128)(2,1)}, bf16[512,768]{1,0:T(8,128)(2,1)}, u32[]{:S(2)}, u32[]{:S(2)}) collective-permute-start(bf16[512,768]{1,0:T(8,128)(2,1)} %bitcast.50.refs_8_), channel_id=1, source_target_pairs={{0,2},{2,0},{4,6},{6,4},{1,3},{3,1},{5,7},{7,5},{8,10},{10,8},{12,... | collective-permute-start | bytes 2359304 | tf_op jit(solution)/shard_map/ppermute | solution.py:87
  107.7 24.7 %collective-permute-start.36 = (bf16[4,384,128]{2,1,0:T(8,128)(2,1)}, bf16[4,384,128]{2,1,0:T(8,128)(2,1)S(1)}, u32[]{:S(2)}, u32[]{:S(2)}) collective-permute-start(bf16[4,384,128]{2,1,0:T(8,128)(2,1)} %collective-permute-done.34), channel_id=1, source_target_pairs={{0,2},{2,0},{4,6},{6,4},{1,3},{3,1},{5,7},{7,5},{8,10},{10,8},{12,... | collective-permute-start | bytes 1179656 | tf_op jit(solution)/shard_map/ppermute | solution.py:87
  135.5 31.8 %collective-permute-start.40 = (bf16[96,2048]{1,0:T(8,128)(2,1)S(1)}, bf16[96,2048]{1,0:T(8,128)(2,1)}, u32[]{:S(2)}, u32[]{:S(2)}) collective-permute-start(bf16[96,2048]{1,0:T(8,128)(2,1)S(1)} %multiply_convert_fusion.refs_2_), channel_id=1, source_target_pairs={{0,16},{8,24},{16,0},{24,8},{1,17},{9,25},{17,1},{25,9},{2,18},{10... | collective-permute-start | bytes 1179656 | tf_op jit(solution)/shard_map/ppermute | solution.py:87
  140.7 29.9 %collective-permute-start.21 = (bf16[512,768]{1,0:T(8,128)(2,1)}, bf16[512,768]{1,0:T(8,128)(2,1)S(1)}, u32[]{:S(2)}, u32[]{:S(2)}) collective-permute-start(bf16[512,768]{1,0:T(8,128)(2,1)} %copy-done.28), channel_id=1, source_target_pairs={{0,4},{2,6},{4,0},{6,2},{1,5},{3,7},{5,1},{7,3},{8,12},{10,14},{12... | collective-permute-start | bytes 2359304 | tf_op jit(solution)/shard_map/ppermute | solution.py:87
  142.2 28.4 %collective-permute-start.27 = (bf16[512,768]{1,0:T(8,128)(2,1)}, bf16[512,768]{1,0:T(8,128)(2,1)S(1)}, u32[]{:S(2)}, u32[]{:S(2)}) collective-permute-start(bf16[512,768]{1,0:T(8,128)(2,1)} %collective-permute-done.26.refs_10_), channel_id=1, source_target_pairs={{0,2},{2,0},{4,6},{6,4},{1,3},{3,1},{5,7},{7,5},{8,10},{10,8},{12,... | collective-permute-start | bytes 2359304 | tf_op jit(solution)/shard_map/ppermute | solution.py:87
  146.0 23.8 %collective-permute-start.13 = (bf16[96,2048]{1,0:T(8,128)(2,1)S(1)}, bf16[96,2048]{1,0:T(8,128)(2,1)S(1)}, u32[]{:S(2)}, u32[]{:S(2)}) collective-permute-start(bf16[96,2048]{1,0:T(8,128)(2,1)S(1)} %multiply_convert_fusion.refs_2_), channel_id=1, source_target_pairs={{0,8},{8,0},{16,24},{24,16},{1,9},{9,1},{17,25},{25,17},{2,10},{10... | collective-permute-start | bytes 1179656 | tf_op jit(solution)/shard_map/ppermute | solution.py:87
  148.6 21.8 %collective-permute-start.39 = (bf16[96,2048]{1,0:T(8,128)(2,1)}, bf16[96,2048]{1,0:T(8,128)(2,1)S(1)}, u32[]{:S(2)}, u32[]{:S(2)}) collective-permute-start(bf16[96,2048]{1,0:T(8,128)(2,1)} %collective-permute-done.38.refs_0_), channel_id=1, source_target_pairs={{0,1},{1,0},{2,3},{3,2},{4,5},{5,4},{6,7},{7,6},{8,9},{9,8},{10,11... | collective-permute-start | bytes 1179656 | tf_op jit(solution)/shard_map/ppermute | solution.py:87
  191.2 33.1 %collective-permute-start.45 = (bf16[96,2048]{1,0:T(8,128)(2,1)S(1)}, bf16[96,2048]{1,0:T(8,128)(2,1)S(1)}, u32[]{:S(2)}, u32[]{:S(2)}) collective-permute-start(bf16[96,2048]{1,0:T(8,128)(2,1)S(1)} %add_convert_fusion.2), channel_id=1, source_target_pairs={{0,16},{8,24},{16,0},{24,8},{1,17},{9,25},{17,1},{25,9},{2,18},{10... | collective-permute-start | bytes 1179656 | tf_op jit(solution)/shard_map/ppermute | solution.py:87
  191.4 32.9 %collective-permute-start.47 = (bf16[96,2048]{1,0:T(8,128)(2,1)S(1)}, bf16[96,2048]{1,0:T(8,128)(2,1)S(1)}, u32[]{:S(2)}, u32[]{:S(2)}) collective-permute-start(bf16[96,2048]{1,0:T(8,128)(2,1)S(1)} %add_convert_fusion.1), channel_id=1, source_target_pairs={{0,8},{8,0},{16,24},{24,16},{1,9},{9,1},{17,25},{25,17},{2,10},{10... | collective-permute-start | bytes 1179656 | tf_op jit(solution)/shard_map/ppermute | solution.py:87
  (56 other events, 746.0 us)

commit v4 on v3

--- a/solution.py
+++ b/solution.py
@@ -52,10 +52,11 @@
 
 def mixer_kernel(pos_ref, *refs, parts):
     xs, refs = refs[:parts], refs[parts:]
-    gates, ups, downs, outs = refs[0:4], refs[4:8], refs[8:12], refs[12:]
+    pieces, outs = [refs[n : n + 4] for n in range(0, 28, 4)], refs[28:]
+    gate_own, gate_rest, up_own, up_rest, down_own, down_low, down_high = pieces
     z_self, p_self, first_unit = pos_ref[0], pos_ref[1], pos_ref[2]
-    block = downs[0].shape[2]
-    span = gates[0].shape[1]
+    block = down_own[0].shape[1]
+    span = gate_own[0].shape[1]
     own = xs[0].shape[0]
     rows = own * parts
 
@@ -69,13 +70,16 @@
             [jnp.concatenate([x_ref[:, lanes(i, j)] for x_ref in xs], axis=0) for j in range(4)],
             axis=1,
         )
-        gate = gate + jnp.dot(x, gates[i][...], preferred_element_type=F32)
-        up = up + jnp.dot(x, ups[i][...], preferred_element_type=F32)
+        gate_w = jnp.concatenate([gate_own[i][...], gate_rest[i][...]], axis=0)
+        up_w = jnp.concatenate([up_own[i][...], up_rest[i][...]], axis=0)
+        gate = gate + jnp.dot(x, gate_w, preferred_element_type=F32)
+        up = up + jnp.dot(x, up_w, preferred_element_type=F32)
     hidden = gate / (1.0 + jnp.exp(-gate)) * up
     keep = lax.broadcasted_iota(jnp.int32, (rows, span), 1) >= first_unit
     hidden = jnp.where(keep, hidden, 0.0).astype(BF)
     for i in range(4):
-        down = jnp.concatenate([downs[i][j] for j in range(4)], axis=1)
+        rest = [jnp.concatenate([down_low[i][j], down_high[i][j]], axis=0) for j in range(3)]
+        down = jnp.concatenate([down_own[i][...]] + rest, axis=1)
         out = jnp.dot(hidden, down, preferred_element_type=F32).astype(BF)
         for j in range(4):
             for n, o_ref in enumerate(outs):
@@ -97,7 +101,12 @@
     z_self = lax.axis_index("z")
     sends = [part(z_self ^ j) for j in range(1, 4)]
     got = [swap(x, "z", j + 1) for j, x in enumerate(sends)]
-    return jnp.stack([part(z_self)] + got)
+    return part(z_self), got
+
+
+def z_exchange_all(part):
+    own, got = z_exchange(part)
+    return jnp.stack([own] + got)
 
 
 def fast_local(
@@ -121,7 +130,7 @@
     def head(x):
         return lambda g: lax.dynamic_slice_in_dim(x, g * VD, VD, 1)
 
-    qkv = z_exchange(lambda g: jnp.stack([head(x)(g) for x in (keys, values, queries)]))
+    qkv = z_exchange_all(lambda g: jnp.stack([head(x)(g) for x in (keys, values, queries)]))
     key_all = jnp.stack(plane_gather(qkv[:, 0], 1))
     value_all = jnp.stack(plane_gather(qkv[:, 1], 2))
 
@@ -131,15 +140,23 @@
     def start(g):
         return jnp.minimum(g * span, units - span)
 
-    gate_mine = z_exchange(lambda g: lax.dynamic_slice_in_dim(gate_weight, start(g), span, 1))
-    up_mine = z_exchange(lambda g: lax.dynamic_slice_in_dim(up_weight, start(g), span, 1))
-    down_mine = z_exchange(lambda g: lax.dynamic_slice_in_dim(down_weight, start(g), span, 0))
-    gates = plane_gather(gate_mine.reshape(-1, span), 1)
-    ups = plane_gather(up_mine.reshape(-1, span), 2)
+    gate_own, gate_got = z_exchange(
+        lambda g: lax.dynamic_slice_in_dim(gate_weight, start(g), span, 1)
+    )
+    up_own, up_got = z_exchange(lambda g: lax.dynamic_slice_in_dim(up_weight, start(g), span, 1))
+    down_own, down_got = z_exchange(
+        lambda g: lax.dynamic_slice_in_dim(down_weight, start(g), span, 0)
+    )
     half = span // 2
-    low = plane_gather(down_mine[:, :half], 1)
-    high = plane_gather(down_mine[:, half:], 2)
-    downs = [jnp.concatenate(pair, axis=1) for pair in zip(low, high)]
+    weights = (
+        plane_gather(gate_own, 1)
+        + plane_gather(jnp.concatenate(gate_got, axis=0), 1)
+        + plane_gather(up_own, 2)
+        + plane_gather(jnp.concatenate(up_got, axis=0), 2)
+        + plane_gather(down_own, 1)
+        + plane_gather(jnp.stack([x[:half] for x in down_got]), 1)
+        + plane_gather(jnp.stack([x[half:] for x in down_got]), 2)
+    )
 
     lam = lax.dynamic_slice_in_dim(lambdas, z_self, 1, 0)
     smem = pl.BlockSpec(memory_space=pltpu.SMEM)
@@ -161,7 +178,7 @@
     )
     place = jnp.stack([z_self, p_self])
     out = attend(place, lam, qkv[:, 2], key_all, value_all, head_gain.reshape(1, VD))
-    back = z_exchange(lambda g: lax.dynamic_index_in_dim(out, g ^ z_self, 0, keepdims=False))
+    back = z_exchange_all(lambda g: lax.dynamic_index_in_dim(out, g ^ z_self, 0, keepdims=False))
     head_out = jnp.concatenate(
         [lax.dynamic_index_in_dim(back, z_self ^ h, 0, keepdims=False) for h in range(4)], axis=1
     )
@@ -177,8 +194,9 @@
     scale = lax.rsqrt(jnp.mean(first * first, axis=-1, keepdims=True) + 1e-06)
     normed = (first * scale * norm_gain).astype(BF)
     mine = [normed] + [None] * 3
-    for j in (3, 2, 1):
-        mine[j] = swap(normed, "z", j)
+    mine[2] = swap(normed, "z", 2)
+    mine[1] = swap(normed, "z", 1)
+    mine[3] = swap(mine[2], "z", 1)
     other = [swap(x, "tp", 1) for x in mine]
     first_unit = z_self * span - start(z_self)
     pos = jnp.stack([z_self, p_self, first_unit])
@@ -189,7 +207,7 @@
         return pl.pallas_call(
             functools.partial(mixer_kernel, parts=len(xs)),
             out_shape=[jax.ShapeDtypeStruct((own_rows, width), BF)] * len(xs),
-            in_specs=[smem] + [vmem] * (12 + len(xs)),
+            in_specs=[smem] + [vmem] * (len(weights) + len(xs)),
             out_specs=[vmem] * len(xs),
             cost_estimate=pl.CostEstimate(
                 flops=6 * tokens * width * span,
@@ -198,23 +216,22 @@
             ),
             compiler_params=pltpu.CompilerParams(vmem_limit_bytes=50 * 1024 * 1024),
             name="mixer",
-        )(pos, *xs, *gates, *ups, *downs)
+        )(pos, *xs, *weights)
 
     def summed(keep, give):
         got = swap(give, "tp", 1)
         return keep.astype(F32) + got.astype(F32)
 
-    far = mix((3, 2))
-    sums = []
-    for n, j in enumerate((3, 2)):
-        part = summed(far[2 * n], far[2 * n + 1]).astype(BF)
-        sums.append(swap(part, "z", j))
+    keep, give = mix((3,))
+    part = summed(keep, give).astype(BF)
+    joined = swap(part, "z", 1)
+    keep, give = mix((2,))
+    part = (summed(keep, give) + joined.astype(F32)).astype(BF)
+    from_two = swap(part, "z", 2)
     near = mix((1, 0))
     part = summed(near[0], near[1]).astype(BF)
-    sums.append(swap(part, "z", 1))
-    mixer = summed(near[2], near[3])
-    for part in sums:
-        mixer = mixer + part.astype(F32)
+    from_one = swap(part, "z", 1)
+    mixer = summed(near[2], near[3]) + from_one.astype(F32) + from_two.astype(F32)
     finished = (first + 0.5 * mixer).astype(BF)
     return lax.all_gather(finished, "tp", axis=0, tiled=True)
 

time: 229 us -> 244 us (1.066)
  waiting for transfers between devices: 102 us -> 112 us
  local copies, waits for them, and re-layouts: 17.3 us -> 25.6 us
  other arithmetic: 12.4 us -> 5.63 us
  Pallas kernels: 21.8 us -> 26.5 us
    unnamed x68 -> x103, local copies, waits for them, and re-layouts: 5.85 us -> 18.8 us
    ppermute x48 -> x57, waiting for transfers between devices: 102 us -> 112 us  [swap(): return lax.ppermute(x, axis, [(i, i ^ bit) for i in range(size)])]
    another operation x6 -> x5, other arithmetic: 6.74 us -> 1.17 us  [the longest x3 1.1 us: z_exchange_all(): return jnp.stack([own] + got)]
    pallas_call x2 -> x3, Pallas kernels: 15.1 us -> 19.6 us  [mix(): pl.pallas_call(functools.partial(mixer_kernel, parts=len(xs)), out_shape=...]
    dynamic_slice x0 -> x3, local copies, waits for them, and re-layouts: none -> 3.88 us  [the longest x1 1.43 us: fast_local(): lax.dynamic_slice_in_dim(down_weight, start(g), span, 0)]
    another operation x3, local copies, waits for them, and re-layouts: 3.25 us -> 0.04 us  [fast_local(): jnp.stack([x[half:] for x in down_got])]
    ppermute x48 -> x57, starting transfers between devices: 71.6 us -> 70 us  [swap(): return lax.ppermute(x, axis, [(i, i ^ bit) for i in range(size)])]
  transfers between devices with their start and end apart: 48 -> 57, of which waited for: 13 -> 22; matrix products, arithmetic and copies ran while one was open for 10% -> 5% of each run, Pallas kernels for 10% -> 11%
where the time goes in v4:
time: 244 us; the launch traced here: 243 us
  waiting for transfers between devices  112 us (46%)
  starting transfers between devices  70 us (29%)
  Pallas kernels  26.5 us (11%)
  local copies, waits for them, and re-layouts  25.6 us (10%)
  other arithmetic  5.63 us (2%)
    ppermute x57, waiting for transfers between devices, swap(): return lax.ppermute(x, axis, [(i, i ^ bit) for i in range(size)])  112 us
    ppermute x57, starting transfers between devices, swap(): return lax.ppermute(x, axis, [(i, i ^ bit) for i in range(size)])  70 us
    pallas_call x3, Pallas kernels, mix(): pl.pallas_call(functools.partial(mixer_kernel, parts=len(xs)), out_shape=...  19.6 us
    unnamed x103, local copies, waits for them, and re-layouts  18.8 us
    pallas_call x1, Pallas kernels, fast_local(): attend(place, lam, qkv[:, 2], key_all, value_all, head_gain.reshape(1, VD))  6.86 us
  transfers between devices with their start and end apart: 57, of which 22 were waited for; matrix products, arithmetic and copies ran while one was open for 5% of the time, Pallas kernels for 11%

profile of v4, /device:TPU:0, one launch (start us, length us, event | category | flops | bytes accessed | tf_op | source)
XLA Modules:
  0.0 243.3 jit_solution(15583481026619141041)
XLA Ops:
  2.8 3.1 %collective-permute-start = (bf16[3,192,128]{2,1,0:T(8,128)(2,1)}, bf16[3,192,128]{2,1,0:T(8,128)(2,1)S(1)}, u32[]{:S(2)}, u32[]{:S(2)}) collective-permute-start(bf16[3,192,128]{2,1,0:T(8,128)(2,1)} %pad_maximum_fusion.6), channel_id=1, source_target_pairs={{0,8},{8,0},{16,24},{24,16},{1,9},{9,1},{17,25},{25,17},{2,10},{10... | collective-permute-start | bytes 442376 | tf_op jit(solution)/shard_map/ppermute | solution.py:91
  6.5 2.6 %collective-permute-start.1 = (bf16[3,192,128]{2,1,0:T(8,128)(2,1)}, bf16[3,192,128]{2,1,0:T(8,128)(2,1)}, u32[]{:S(2)}, u32[]{:S(2)}) collective-permute-start(bf16[3,192,128]{2,1,0:T(8,128)(2,1)} %pad_maximum_fusion.7), channel_id=1, source_target_pairs={{0,16},{8,24},{16,0},{24,8},{1,17},{9,25},{17,1},{25,9},{2,18},{10... | collective-permute-start | bytes 442376 | tf_op jit(solution)/shard_map/ppermute | solution.py:91
  17.3 3.3 %collective-permute-done.1 = bf16[3,192,128]{2,1,0:T(8,128)(2,1)} collective-permute-done((bf16[3,192,128]{2,1,0:T(8,128)(2,1)}, bf16[3,192,128]{2,1,0:T(8,128)(2,1)}, u32[]{:S(2)}, u32[]{:S(2)}) %collective-permute-start.1) | collective-permute-done | bytes 147488 | tf_op jit(solution)/shard_map/ppermute | solution.py:91
  24.3 9.9 %collective-permute-done.37 = bf16[768,128]{1,0:T(8,128)(2,1)S(1)} collective-permute-done((bf16[768,128]{1,0:T(8,128)(2,1)S(1)}, bf16[768,128]{1,0:T(8,128)(2,1)S(1)}, u32[]{:S(2)}, u32[]{:S(2)}) %collective-permute-start.37) | collective-permute-done | bytes 196640 | tf_op jit(solution)/shard_map/ppermute | solution.py:91
  53.7 5.3 %collective-permute-start.20 = (bf16[128,768]{1,0:T(8,128)(2,1)S(1)}, bf16[128,768]{1,0:T(8,128)(2,1)S(1)}, u32[]{:S(2)}, u32[]{:S(2)}) collective-permute-start(bf16[128,768]{1,0:T(8,128)(2,1)S(1)} %copy-done.46), channel_id=1, source_target_pairs={{0,16},{8,24},{16,0},{24,8},{1,17},{9,25},{17,1},{25,9},{2,18},{10... | collective-permute-start | bytes 589832 | tf_op jit(solution)/shard_map/ppermute | solution.py:91
  59.2 6.9 %attn.1 = bf16[4,192,128]{2,1,0:T(8,128)(2,1)S(1)} custom-call(s32[2]{0:T(128)S(1)} %pad_add_fusion.pos_ref, f32[1]{0:T(128)} %dynamic_slice.110.lam_ref, bf16[4,192,128]{2,1,0:T(8,128)(2,1)S(1)} %get-tuple-element.37.q_ref, bf16[4,4,192,128]{3,2,1,0:T(8,128)(2,1)S(1)} %pad_maximum_fusion.k_ref, bf16[4,4,192,128]{3,2,1,0:T(8,128)(2,1)S(1)} %pad_maximum_fusion.1.v_ref, ...), custom_call_target="tpu_custom_call" | custom-call | flops 1811939328 | bytes 1572864 | tf_op jit(solution)/shard_map/attn/pallas_call | solution.py:180
  66.1 2.7 %collective-permute-start.9 = (bf16[192,128]{1,0:T(8,128)(2,1)S(1)}, bf16[192,128]{1,0:T(8,128)(2,1)S(1)}, u32[]{:S(2)}, u32[]{:S(2)}) collective-permute-start(bf16[192,128]{1,0:T(8,128)(2,1)S(1)} %get-tuple-element.51), channel_id=1, source_target_pairs={{0,8},{8,0},{16,24},{24,16},{1,9},{9,1},{17,25},{25,17},{2,10},{10... | collective-permute-start | bytes 147464 | tf_op jit(solution)/shard_map/ppermute | solution.py:91
  73.9 9.5 %collective-permute-done.10 = bf16[192,128]{1,0:T(8,128)(2,1)S(1)} collective-permute-done((bf16[192,128]{1,0:T(8,128)(2,1)S(1)}, bf16[192,128]{1,0:T(8,128)(2,1)S(1)}, u32[]{:S(2)}, u32[]{:S(2)}) %collective-permute-start.10) | collective-permute-done | bytes 49184 | tf_op jit(solution)/shard_map/ppermute | solution.py:91
  85.9 11.2 %collective-permute-done.29 = bf16[128,768]{1,0:T(8,128)(2,1)S(1)} collective-permute-done((bf16[128,768]{1,0:T(8,128)(2,1)S(1)}, bf16[128,768]{1,0:T(8,128)(2,1)S(1)}, u32[]{:S(2)}, u32[]{:S(2)}) %collective-permute-start.29) | collective-permute-done | bytes 196640 | tf_op jit(solution)/shard_map/ppermute | solution.py:91
  106.3 4.5 %collective-permute-done.34.refs_21_.refs_19_ = bf16[768,128]{1,0:T(8,128)(2,1)S(1)} collective-permute-done((bf16[768,128]{1,0:T(8,128)(2,1)S(1)}, bf16[768,128]{1,0:T(8,128)(2,1)S(1)}, u32[]{:S(2)}, u32[]{:S(2)}) %collective-permute-start.34) | collective-permute-done | bytes 196640 | tf_op jit(solution)/shard_map/ppermute | solution.py:91
  115.5 3.1 %collective-permute-done.18.refs_7_.refs_5_ = bf16[128,768]{1,0:T(8,128)(2,1)S(1)} collective-permute-done((bf16[128,768]{1,0:T(8,128)(2,1)S(1)}, bf16[128,768]{1,0:T(8,128)(2,1)S(1)}, u32[]{:S(2)}, u32[]{:S(2)}) %collective-permute-start.18) | collective-permute-done | bytes 196640 | tf_op jit(solution)/shard_map/ppermute | solution.py:91
  126.4 9.0 %collective-permute-done.44.refs_30_.refs_28_ = bf16[3,384,128]{2,1,0:T(8,128)(2,1)S(1)} collective-permute-done((bf16[3,384,128]{2,1,0:T(8,128)(2,1)S(1)}, bf16[3,384,128]{2,1,0:T(8,128)(2,1)S(1)}, u32[]{:S(2)}, u32[]{:S(2)}) %collective-permute-start.44) | collective-permute-done | bytes 294944 | tf_op jit(solution)/shard_map/ppermute | solution.py:91
  136.6 2.7 %collective-permute-start.49 = (bf16[96,2048]{1,0:T(8,128)(2,1)}, bf16[96,2048]{1,0:T(8,128)(2,1)S(1)}, u32[]{:S(2)}, u32[]{:S(2)}) collective-permute-start(bf16[96,2048]{1,0:T(8,128)(2,1)} %multiply_convert_fusion.refs_2_), channel_id=1, source_target_pairs={{0,16},{8,24},{16,0},{24,8},{1,17},{9,25},{17,1},{25,9},{2,18},{10... | collective-permute-start | bytes 1179656 | tf_op jit(solution)/shard_map/ppermute | solution.py:91
  142.7 6.5 %collective-permute-done.49.refs_0_ = bf16[96,2048]{1,0:T(8,128)(2,1)S(1)} collective-permute-done((bf16[96,2048]{1,0:T(8,128)(2,1)}, bf16[96,2048]{1,0:T(8,128)(2,1)S(1)}, u32[]{:S(2)}, u32[]{:S(2)}) %collective-permute-start.49) | collective-permute-done | bytes 393248 | tf_op jit(solution)/shard_map/ppermute | solution.py:91
  149.2 2.9 %collective-permute-start.52 = (bf16[96,2048]{1,0:T(8,128)(2,1)S(1)}, bf16[96,2048]{1,0:T(8,128)(2,1)}, u32[]{:S(2)}, u32[]{:S(2)}) collective-permute-start(bf16[96,2048]{1,0:T(8,128)(2,1)S(1)} %collective-permute-done.49.refs_0_), channel_id=1, source_target_pairs={{0,8},{8,0},{16,24},{24,16},{1,9},{9,1},{17,25},{25,17},{2,10},{10... | collective-permute-start | bytes 1179656 | tf_op jit(solution)/shard_map/ppermute | solution.py:91
  152.2 8.5 %collective-permute-done.23.refs_10_.refs_8_ = bf16[384,768]{1,0:T(8,128)(2,1)S(1)} collective-permute-done((bf16[384,768]{1,0:T(8,128)(2,1)S(1)}, bf16[384,768]{1,0:T(8,128)(2,1)S(1)}, u32[]{:S(2)}, u32[]{:S(2)}) %collective-permute-start.23) | collective-permute-done | bytes 589856 | tf_op jit(solution)/shard_map/ppermute | solution.py:91
  162.7 3.3 %collective-permute-done.42.refs_27_.refs_25_ = bf16[3,384,128]{2,1,0:T(8,128)(2,1)S(1)} collective-permute-done((bf16[3,384,128]{2,1,0:T(8,128)(2,1)S(1)}, bf16[3,384,128]{2,1,0:T(8,128)(2,1)S(1)}, u32[]{:S(2)}, u32[]{:S(2)}) %collective-permute-start.42) | collective-permute-done | bytes 294944 | tf_op jit(solution)/shard_map/ppermute | solution.py:91
  168.3 6.1 %collective-permute-done.45.refs_31_.refs_29_ = bf16[3,384,128]{2,1,0:T(8,128)(2,1)S(1)} collective-permute-done((bf16[3,384,128]{2,1,0:T(8,128)(2,1)S(1)}, bf16[3,384,128]{2,1,0:T(8,128)(2,1)S(1)}, u32[]{:S(2)}, u32[]{:S(2)}) %collective-permute-start.45) | collective-permute-done | bytes 294944 | tf_op jit(solution)/shard_map/ppermute | solution.py:91
  186.1 5.8 %mixer.5 = (bf16[96,2048]{1,0:T(8,128)(2,1)}, bf16[96,2048]{1,0:T(8,128)(2,1)}) custom-call(s32[3]{0:T(128)S(1)} %pad_add_fusion.1.pos_ref, bf16[96,2048]{1,0:T(8,128)(2,1)} %collective-permute-done.52.refs_0_, bf16[96,2048]{1,0:T(8,128)(2,1)} %collective-permute-done.53.refs_1_, bf16[128,768]{1,0:T(8,128)(2,1)S(1)} %get-tuple-element.31.refs_4_.refs_2_, ...), custom_call_target="tpu_custom_call" | custom-call | flops 1811939328 | bytes 11010048 | tf_op jit(solution)/shard_map/mixer/pallas_call | solution.py:207
  191.9 8.1 %mixer.3 = (bf16[96,2048]{1,0:T(8,128)(2,1)}, bf16[96,2048]{1,0:T(8,128)(2,1)}, bf16[96,2048]{1,0:T(8,128)(2,1)}, bf16[96,2048]{1,0:T(8,128)(2,1)}) custom-call(s32[3]{0:T(128)S(1)} %pad_add_fusion.1.pos_ref, bf16[96,2048]{1,0:T(8,128)(2,1)} %collective-permute-done.13.refs_0_, bf16[96,2048]{1,0:T(8,128)(2,1)} %collective-permute-done.14.refs_1_, ...), custom_call_target="tpu_custom_call" | custom-call | flops 3623878656 | bytes 12582912 | tf_op jit(solution)/shard_map/mixer/pallas_call | solution.py:207
  201.2 5.8 %mixer.4 = (bf16[96,2048]{1,0:T(8,128)(2,1)}, bf16[96,2048]{1,0:T(8,128)(2,1)}) custom-call(s32[3]{0:T(128)S(1)} %pad_add_fusion.1.pos_ref, bf16[96,2048]{1,0:T(8,128)(2,1)} %copy-done.39, bf16[96,2048]{1,0:T(8,128)(2,1)} %copy-done.40, bf16[128,768]{1,0:T(8,128)(2,1)S(1)} %get-tuple-element.31.refs_4_.refs_2_, ...), custom_call_target="tpu_custom_call" | custom-call | flops 1811939328 | bytes 11010048 | tf_op jit(solution)/shard_map/mixer/pallas_call | solution.py:207
  210.3 9.8 %collective-permute-done.55 = bf16[96,2048]{1,0:T(8,128)(2,1)S(1)} collective-permute-done((bf16[96,2048]{1,0:T(8,128)(2,1)S(1)}, bf16[96,2048]{1,0:T(8,128)(2,1)S(1)}, u32[]{:S(2)}, u32[]{:S(2)}) %collective-permute-start.55) | collective-permute-done | bytes 393248 | tf_op jit(solution)/shard_map/ppermute | solution.py:91
  222.7 12.0 %collective-permute-done.48 = bf16[96,2048]{1,0:T(8,128)(2,1)S(1)} collective-permute-done((bf16[96,2048]{1,0:T(8,128)(2,1)S(1)}, bf16[96,2048]{1,0:T(8,128)(2,1)S(1)}, u32[]{:S(2)}, u32[]{:S(2)}) %collective-permute-start.48) | collective-permute-done | bytes 393248 | tf_op jit(solution)/shard_map/ppermute | solution.py:91
  234.7 4.9 %collective-permute-done.56 = bf16[96,2048]{1,0:T(8,128)(2,1)S(1)} collective-permute-done((bf16[96,2048]{1,0:T(8,128)(2,1)S(1)}, bf16[96,2048]{1,0:T(8,128)(2,1)S(1)}, u32[]{:S(2)}, u32[]{:S(2)}) %collective-permute-start.56) | collective-permute-done | bytes 393248 | tf_op jit(solution)/shard_map/ppermute | solution.py:91
  (233 shorter events, 95.6 us)
Async XLA Ops:
  11.0 30.1 %collective-permute-start.19 = (bf16[128,768]{1,0:T(8,128)(2,1)}, bf16[128,768]{1,0:T(8,128)(2,1)}, u32[]{:S(2)}, u32[]{:S(2)}) collective-permute-start(bf16[128,768]{1,0:T(8,128)(2,1)} %get-tuple-element.30), channel_id=1, source_target_pairs={{0,8},{8,0},{16,24},{24,16},{1,9},{9,1},{17,25},{25,17},{2,10},{10... | collective-permute-start | bytes 589832 | tf_op jit(solution)/shard_map/ppermute | solution.py:91
  13.1 31.0 %collective-permute-start.28 = (bf16[128,768]{1,0:T(8,128)(2,1)}, bf16[128,768]{1,0:T(8,128)(2,1)}, u32[]{:S(2)}, u32[]{:S(2)}) collective-permute-start(bf16[128,768]{1,0:T(8,128)(2,1)} %get-tuple-element.26), channel_id=1, source_target_pairs={{0,8},{8,0},{16,24},{24,16},{1,9},{9,1},{17,25},{25,17},{2,10},{10... | collective-permute-start | bytes 589832 | tf_op jit(solution)/shard_map/ppermute | solution.py:91
  16.4 17.8 %collective-permute-start.37 = (bf16[768,128]{1,0:T(8,128)(2,1)S(1)}, bf16[768,128]{1,0:T(8,128)(2,1)S(1)}, u32[]{:S(2)}, u32[]{:S(2)}) collective-permute-start(bf16[768,128]{1,0:T(8,128)(2,1)S(1)} %get-tuple-element.21), channel_id=1, source_target_pairs={{0,8},{8,0},{16,24},{24,16},{1,9},{9,1},{17,25},{25,17},{2,10},{10... | collective-permute-start | bytes 589832 | tf_op jit(solution)/shard_map/ppermute | solution.py:91
  20.8 18.6 %collective-permute-start.39 = (bf16[768,128]{1,0:T(8,128)(2,1)S(1)}, bf16[768,128]{1,0:T(8,128)(2,1)S(1)}, u32[]{:S(2)}, u32[]{:S(2)}) collective-permute-start(bf16[768,128]{1,0:T(8,128)(2,1)S(1)} %get-tuple-element.23), channel_id=1, source_target_pairs={{0,24},{8,16},{16,8},{24,0},{1,25},{9,17},{17,9},{25,1},{2,26},{10... | collective-permute-start | bytes 589832 | tf_op jit(solution)/shard_map/ppermute | solution.py:91
  34.2 66.0 %collective-permute-start.16 = (bf16[128,768]{1,0:T(8,128)(2,1)S(1)}, bf16[128,768]{1,0:T(8,128)(2,1)S(1)}, u32[]{:S(2)}, u32[]{:S(2)}) collective-permute-start(bf16[128,768]{1,0:T(8,128)(2,1)S(1)} %get-tuple-element.31.refs_4_.refs_2_), channel_id=1, source_target_pairs={{0,2},{2,0},{4,6},{6,4},{1,3},{3,1},{5,7},{7,5},{8,10},{10,8},{12,... | collective-permute-start | bytes 589832 | tf_op jit(solution)/shard_map/ppermute | solution.py:91
  51.5 59.8 %collective-permute-start.17 = (bf16[128,768]{1,0:T(8,128)(2,1)S(1)}, bf16[128,768]{1,0:T(8,128)(2,1)S(1)}, u32[]{:S(2)}, u32[]{:S(2)}) collective-permute-start(bf16[128,768]{1,0:T(8,128)(2,1)S(1)} %get-tuple-element.31.refs_4_.refs_2_), channel_id=1, source_target_pairs={{0,4},{2,6},{4,0},{6,2},{1,5},{3,7},{5,1},{7,3},{8,12},{10,14},{12... | collective-permute-start | bytes 589832 | tf_op jit(solution)/shard_map/ppermute | solution.py:91
  53.7 16.3 %collective-permute-start.20 = (bf16[128,768]{1,0:T(8,128)(2,1)S(1)}, bf16[128,768]{1,0:T(8,128)(2,1)S(1)}, u32[]{:S(2)}, u32[]{:S(2)}) collective-permute-start(bf16[128,768]{1,0:T(8,128)(2,1)S(1)} %copy-done.46), channel_id=1, source_target_pairs={{0,16},{8,24},{16,0},{24,8},{1,17},{9,25},{17,1},{25,9},{2,18},{10... | collective-permute-start | bytes 589832 | tf_op jit(solution)/shard_map/ppermute | solution.py:91
  100.8 24.1 %collective-permute-start.40 = (bf16[3,384,128]{2,1,0:T(8,128)(2,1)S(1)}, bf16[3,384,128]{2,1,0:T(8,128)(2,1)S(1)}, u32[]{:S(2)}, u32[]{:S(2)}) collective-permute-start(bf16[3,384,128]{2,1,0:T(8,128)(2,1)S(1)} %pad_maximum_fusion.3.refs_24_.refs_22_), channel_id=1, source_target_pairs={{0,2},{2,0},{4,6},{6,4},{1,3},{3,1},{5,7},{7,5},{8,10},{10,8},{12,... | collective-permute-start | bytes 884744 | tf_op jit(solution)/shard_map/ppermute | solution.py:91
  115.0 20.9 %collective-permute-start.41 = (bf16[3,384,128]{2,1,0:T(8,128)(2,1)S(1)}, bf16[3,384,128]{2,1,0:T(8,128)(2,1)S(1)}, u32[]{:S(2)}, u32[]{:S(2)}) collective-permute-start(bf16[3,384,128]{2,1,0:T(8,128)(2,1)S(1)} %pad_maximum_fusion.3.refs_24_.refs_22_), channel_id=1, source_target_pairs={{0,4},{2,6},{4,0},{6,2},{1,5},{3,7},{5,1},{7,3},{8,12},{10,14},{12... | collective-permute-start | bytes 884744 | tf_op jit(solution)/shard_map/ppermute | solution.py:91
  119.2 16.2 %collective-permute-start.44 = (bf16[3,384,128]{2,1,0:T(8,128)(2,1)S(1)}, bf16[3,384,128]{2,1,0:T(8,128)(2,1)S(1)}, u32[]{:S(2)}, u32[]{:S(2)}) collective-permute-start(bf16[3,384,128]{2,1,0:T(8,128)(2,1)S(1)} %pad_maximum_fusion.4.refs_28_.refs_26_), channel_id=1, source_target_pairs={{0,4},{2,6},{4,0},{6,2},{1,5},{3,7},{5,1},{7,3},{8,12},{10,14},{12... | collective-permute-start | bytes 884744 | tf_op jit(solution)/shard_map/ppermute | solution.py:91
  120.4 18.9 %collective-permute-start.43 = (bf16[3,384,128]{2,1,0:T(8,128)(2,1)S(1)}, bf16[3,384,128]{2,1,0:T(8,128)(2,1)S(1)}, u32[]{:S(2)}, u32[]{:S(2)}) collective-permute-start(bf16[3,384,128]{2,1,0:T(8,128)(2,1)S(1)} %pad_maximum_fusion.4.refs_28_.refs_26_), channel_id=1, source_target_pairs={{0,2},{2,0},{4,6},{6,4},{1,3},{3,1},{5,7},{7,5},{8,10},{10,8},{12,... | collective-permute-start | bytes 884744 | tf_op jit(solution)/shard_map/ppermute | solution.py:91
  123.4 18.4 %collective-permute-start.22 = (bf16[384,768]{1,0:T(8,128)(2,1)S(1)}, bf16[384,768]{1,0:T(8,128)(2,1)}, u32[]{:S(2)}, u32[]{:S(2)}) collective-permute-start(bf16[384,768]{1,0:T(8,128)(2,1)S(1)} %constant_dynamic-update-slice_fusion.refs_8_.refs_6_), channel_id=1, source_target_pairs={{0,2},{2,0},{4,6},{6,4},{1,3},{3,1},{5,7},{7,5},{8,10},{10,8},{12,... | collective-permute-start | bytes 1769480 | tf_op jit(solution)/shard_map/ppermute | solution.py:91
  124.9 27.2 %collective-permute-start.32 = (bf16[384,768]{1,0:T(8,128)(2,1)S(1)}, bf16[384,768]{1,0:T(8,128)(2,1)}, u32[]{:S(2)}, u32[]{:S(2)}) collective-permute-start(bf16[384,768]{1,0:T(8,128)(2,1)S(1)} %constant_dynamic-update-slice_fusion.3.refs_16_.refs_14_), channel_id=1, source_target_pairs={{0,4},{2,6},{4,0},{6,2},{1,5},{3,7},{5,1},{7,3},{8,12},{10,14},{12... | collective-permute-start | bytes 1769480 | tf_op jit(solution)/shard_map/ppermute | solution.py:91
  135.4 25.3 %collective-permute-start.23 = (bf16[384,768]{1,0:T(8,128)(2,1)S(1)}, bf16[384,768]{1,0:T(8,128)(2,1)S(1)}, u32[]{:S(2)}, u32[]{:S(2)}) collective-permute-start(bf16[384,768]{1,0:T(8,128)(2,1)S(1)} %constant_dynamic-update-slice_fusion.refs_8_.refs_6_), channel_id=1, source_target_pairs={{0,4},{2,6},{4,0},{6,2},{1,5},{3,7},{5,1},{7,3},{8,12},{10,14},{12... | collective-permute-start | bytes 1769480 | tf_op jit(solution)/shard_map/ppermute | solution.py:91
  139.3 21.8 %collective-permute-start.31 = (bf16[384,768]{1,0:T(8,128)(2,1)S(1)}, bf16[384,768]{1,0:T(8,128)(2,1)S(1)}, u32[]{:S(2)}, u32[]{:S(2)}) collective-permute-start(bf16[384,768]{1,0:T(8,128)(2,1)S(1)} %constant_dynamic-update-slice_fusion.3.refs_16_.refs_14_), channel_id=1, source_target_pairs={{0,2},{2,0},{4,6},{6,4},{1,3},{3,1},{5,7},{7,5},{8,10},{10,8},{12,... | collective-permute-start | bytes 1769480 | tf_op jit(solution)/shard_map/ppermute | solution.py:91
  141.8 24.1 %collective-permute-start.42 = (bf16[3,384,128]{2,1,0:T(8,128)(2,1)S(1)}, bf16[3,384,128]{2,1,0:T(8,128)(2,1)S(1)}, u32[]{:S(2)}, u32[]{:S(2)}) collective-permute-start(bf16[3,384,128]{2,1,0:T(8,128)(2,1)S(1)} %collective-permute-done.40.refs_25_.refs_23_), channel_id=1, source_target_pairs={{0,4},{2,6},{4,0},{6,2},{1,5},{3,7},{5,1},{7,3},{8,12},{10,14},{12... | collective-permute-start | bytes 884744 | tf_op jit(solution)/shard_map/ppermute | solution.py:91
  149.2 19.1 %collective-permute-start.52 = (bf16[96,2048]{1,0:T(8,128)(2,1)S(1)}, bf16[96,2048]{1,0:T(8,128)(2,1)}, u32[]{:S(2)}, u32[]{:S(2)}) collective-permute-start(bf16[96,2048]{1,0:T(8,128)(2,1)S(1)} %collective-permute-done.49.refs_0_), channel_id=1, source_target_pairs={{0,8},{8,0},{16,24},{24,16},{1,9},{9,1},{17,25},{25,17},{2,10},{10... | collective-permute-start | bytes 1179656 | tf_op jit(solution)/shard_map/ppermute | solution.py:91
  152.1 22.4 %collective-permute-start.13 = (bf16[96,2048]{1,0:T(8,128)(2,1)}, bf16[96,2048]{1,0:T(8,128)(2,1)}, u32[]{:S(2)}, u32[]{:S(2)}) collective-permute-start(bf16[96,2048]{1,0:T(8,128)(2,1)} %multiply_convert_fusion.refs_2_), channel_id=1, source_target_pairs={{0,8},{8,0},{16,24},{24,16},{1,9},{9,1},{17,25},{25,17},{2,10},{10... | collective-permute-start | bytes 1179656 | tf_op jit(solution)/shard_map/ppermute | solution.py:91
  174.4 17.4 %collective-permute-start.15 = (bf16[96,2048]{1,0:T(8,128)(2,1)}, bf16[96,2048]{1,0:T(8,128)(2,1)}, u32[]{:S(2)}, u32[]{:S(2)}) collective-permute-start(bf16[96,2048]{1,0:T(8,128)(2,1)} %multiply_convert_fusion.refs_2_), channel_id=1, source_target_pairs={{0,1},{1,0},{2,3},{3,2},{4,5},{5,4},{6,7},{7,6},{8,9},{9,8},{10,11... | collective-permute-start | bytes 1179656 | tf_op jit(solution)/shard_map/ppermute | solution.py:91
  175.2 16.7 %collective-permute-start.14 = (bf16[96,2048]{1,0:T(8,128)(2,1)}, bf16[96,2048]{1,0:T(8,128)(2,1)}, u32[]{:S(2)}, u32[]{:S(2)}) collective-permute-start(bf16[96,2048]{1,0:T(8,128)(2,1)} %collective-permute-done.13.refs_0_), channel_id=1, source_target_pairs={{0,1},{1,0},{2,3},{3,2},{4,5},{5,4},{6,7},{7,6},{8,9},{9,8},{10,11... | collective-permute-start | bytes 1179656 | tf_op jit(solution)/shard_map/ppermute | solution.py:91
  175.2 25.2 %collective-permute-start.50 = (bf16[96,2048]{1,0:T(8,128)(2,1)}, bf16[96,2048]{1,0:T(8,128)(2,1)S(1)}, u32[]{:S(2)}, u32[]{:S(2)}) collective-permute-start(bf16[96,2048]{1,0:T(8,128)(2,1)} %copy-done.39), channel_id=1, source_target_pairs={{0,1},{1,0},{2,3},{3,2},{4,5},{5,4},{6,7},{7,6},{8,9},{9,8},{10,11... | collective-permute-start | bytes 1179656 | tf_op jit(solution)/shard_map/ppermute | solution.py:91
  200.4 22.3 %collective-permute-start.46 = (bf16[96,2048]{1,0:T(8,128)(2,1)}, bf16[96,2048]{1,0:T(8,128)(2,1)S(1)}, u32[]{:S(2)}, u32[]{:S(2)}) collective-permute-start(bf16[96,2048]{1,0:T(8,128)(2,1)} %get-tuple-element.14), channel_id=1, source_target_pairs={{0,1},{1,0},{2,3},{3,2},{4,5},{5,4},{6,7},{7,6},{8,9},{9,8},{10,11... | collective-permute-start | bytes 1179656 | tf_op jit(solution)/shard_map/ppermute | solution.py:91
  210.2 24.5 %collective-permute-start.48 = (bf16[96,2048]{1,0:T(8,128)(2,1)S(1)}, bf16[96,2048]{1,0:T(8,128)(2,1)S(1)}, u32[]{:S(2)}, u32[]{:S(2)}) collective-permute-start(bf16[96,2048]{1,0:T(8,128)(2,1)S(1)} %add_convert_fusion.3), channel_id=1, source_target_pairs={{0,8},{8,0},{16,24},{24,16},{1,9},{9,1},{17,25},{25,17},{2,10},{10... | collective-permute-start | bytes 1179656 | tf_op jit(solution)/shard_map/ppermute | solution.py:91
  220.2 19.4 %collective-permute-start.56 = (bf16[96,2048]{1,0:T(8,128)(2,1)S(1)}, bf16[96,2048]{1,0:T(8,128)(2,1)S(1)}, u32[]{:S(2)}, u32[]{:S(2)}) collective-permute-start(bf16[96,2048]{1,0:T(8,128)(2,1)S(1)} %add_convert_fusion.1), channel_id=1, source_target_pairs={{0,16},{8,24},{16,0},{24,8},{1,17},{9,25},{17,1},{25,9},{2,18},{10... | collective-permute-start | bytes 1179656 | tf_op jit(solution)/shard_map/ppermute | solution.py:91
  (82 other events, 1428.1 us)
